TPU v7x, 256 devices: a whole 4x4x8 slice. The times are simulated.
256 devices in a mesh: sp: 32 (over z, x), tp: 8 (over y, core).
Axes of the slice: x: 4, y: 4, z: 8, core: 2. Of those that a mesh axis runs over, the one named last changes fastest.
Arguments:
- tokens: bfloat16 [24576, 2048], P(('sp', 'tp')), may hold values from -6 to 6
- in_gain: float32 [2048], replicated, may hold values from 0.1 to 1.9
- w_query: bfloat16 [2048, 1024], P(None, 'tp'), may hold values from -0.125 to 0.125
- w_key: bfloat16 [2048, 1024], P(None, 'tp'), may hold values from -0.125 to 0.125
- w_value: bfloat16 [2048, 2048], P(None, 'tp'), may hold values from -0.125 to 0.125
- w_input_gate: bfloat16 [2048, 8], replicated, may hold values from -8 to 8
- w_forget_gate: bfloat16 [2048, 8], replicated, may hold values from -0.125 to 0.125
- forget_bias: float32 [8], replicated
- forget_extra: float32 [24576, 8], P('sp', 'tp'), may hold values from -2 to 0
- w_conv_gate: bfloat16 [2048, 2048], P(None, 'tp'), may hold values from -0.125 to 0.125
- w_conv_left: bfloat16 [2048, 2048], P(None, 'tp'), may hold values from -0.125 to 0.125
- w_conv_right: bfloat16 [2048, 2048], P(None, 'tp'), may hold values from -0.125 to 0.125
- conv_taps: float32 [3, 2048], replicated, may hold values from -3.5 to 3.5
- first_memory: float32 [8, 128, 256], P('tp'), may hold values from -5120 to 5120
- first_norm: float32 [8, 128], P('tp'), may hold values from -5120 to 5120
- w_out_memory: bfloat16 [2048, 2048], P('tp'), may hold values from -0.09375 to 0.09375
- w_out_conv: bfloat16 [2048, 2048], P('tp'), may hold values from -0.09375 to 0.09375
Outputs:
- mixed: bfloat16 [24576, 2048], P(('sp', 'tp'))
All inputs are finite; a program needn't handle non-finite values.
Results may differ from a plain program's by a relative error of at most 0.015.
The roundings to bfloat16 on the way count: a program that leaves them out, or rounds other values in their place, can miss the bound.
Values may be sent and summed in bfloat16 or wider, within the bound.
A program may use at most 64 MiB of HBM per device.

v0:
```python
import jax
import jax.numpy as jnp
from jax import lax
from jax.sharding import Mesh
from jax.sharding import PartitionSpec as P

KEY_DIM = 128
VALUE_DIM = 256
TAPS = 3
V_WIDTH = 2048
SP = ("sp_0", "sp_1")
SP_TP = ("sp_0", "sp_1", "tp")


epsilon = 1e-06
very_negative = -1e30
highest = lax.Precision.HIGHEST


def from_behind(block, axis, distance):
    devices = range(lax.axis_size(axis))
    route = [(i - distance, i) for i in devices if i - distance in devices]
    return lax.ppermute(block, axis, route)


def filled_with(x, identity):
    return jax.tree.map(
        lambda part, zero: jnp.zeros_like(part) + jnp.asarray(zero, part.dtype), x, identity
    )


def collected_together(x, axis):
    leaves = jax.tree.leaves(x)
    sequence = sorted(range(len(leaves)), key=lambda k: -leaves[k].size)
    width = (1, *leaves[sequence[0]].shape)[-1]
    lines = [
        jnp.pad(leaves[k].reshape(-1), (0, -leaves[k].size % width)).reshape(-1, width)
        for k in sequence
    ]
    both, at, found = (lax.all_gather(jnp.concatenate(lines), axis), 0, {})
    for k, line in zip(sequence, lines):
        slab = both[:, at : at + len(line)].reshape(len(both), -1)
        found[k] = slab[:, : leaves[k].size].reshape(-1, *leaves[k].shape)
        at += len(line)
    numbers = iter(range(len(leaves)))
    return jax.tree.map(lambda _: found[next(numbers)], x)


def entering(x, axes, combine, identity):
    before = start = filled_with(x, identity)
    running = x
    for axis in reversed(axes):
        size, here = (lax.axis_size(axis), lax.axis_index(axis))
        pieces = collected_together(running, axis)
        inside, running = (start, start)
        for k in range(size):
            passed = k < here
            running = combine(running, jax.tree.map(lambda part: part[k], pieces))
            inside = jax.tree.map(lambda new, old: jnp.where(passed, new, old), running, inside)
        before = combine(inside, before)
    return before


def rounded(values):
    return lax.optimization_barrier(values.astype(jnp.bfloat16)).astype(jnp.float32)


def join_states(earlier, later):
    decay_early, max_early, memory_early, norm_early = earlier
    decay_late, max_late, memory_late, norm_late = later
    joined_max = jnp.maximum(max_early + decay_late, max_late)
    scale_early = jnp.exp(max_early + decay_late - joined_max)
    scale_late = jnp.exp(max_late - joined_max)
    joined_memory = (
        scale_early[:, None, None] * memory_early + scale_late[:, None, None] * memory_late
    )
    joined_norm = scale_early[:, None] * norm_early + scale_late[:, None] * norm_late
    return (decay_early + decay_late, joined_max, joined_memory, joined_norm)


def per_device(
    tokens,
    in_gain,
    w_query,
    w_key,
    w_value,
    w_input_gate,
    w_forget_gate,
    forget_bias,
    forget_extra,
    w_conv_gate,
    w_conv_left,
    w_conv_right,
    conv_taps,
    first_memory,
    first_norm,
    w_out_memory,
    w_out_conv,
):
    heads_here = w_query.shape[1] // KEY_DIM
    query_width = heads_here * KEY_DIM
    value_width = heads_here * VALUE_DIM
    channels = w_conv_gate.shape[1]
    head_first = lax.axis_index("tp") * heads_here
    channel_first = lax.axis_index("tp") * channels
    input_gate = lax.dynamic_slice_in_dim(w_input_gate, head_first, heads_here, 1)
    forget_gate = lax.dynamic_slice_in_dim(w_forget_gate, head_first, heads_here, 1)
    bias_here = lax.dynamic_slice_in_dim(forget_bias, head_first, heads_here, 0)
    taps_here = lax.dynamic_slice_in_dim(conv_taps, channel_first, channels, 1)
    token_rows = tokens.astype(jnp.float32)
    scale_rows = lax.rsqrt(jnp.mean(token_rows * token_rows, axis=1, keepdims=True) + epsilon)
    normed = (token_rows * scale_rows * in_gain).astype(jnp.bfloat16)
    sub_rows = lax.all_gather(normed, "tp", axis=0, tiled=True)
    pieces = [
        jnp.dot(sub_rows, weight, preferred_element_type=jnp.float32)
        for weight in (
            w_query,
            w_key,
            w_value,
            w_conv_gate,
            w_conv_left,
            w_conv_right,
            input_gate,
            forget_gate,
        )
    ]
    projected = jnp.concatenate(pieces, axis=1)
    row_count = projected.shape[0]
    offset_value = 2 * query_width
    offset_conv = offset_value + value_width
    offset_gate = offset_conv + 3 * channels
    query_rows = (
        projected[:, 0:query_width].astype(jnp.bfloat16).reshape(row_count, heads_here, KEY_DIM)
    )
    key_rows = (
        projected[:, query_width:offset_value]
        .astype(jnp.bfloat16)
        .reshape(row_count, heads_here, KEY_DIM)
    )
    value_rows = (
        projected[:, offset_value:offset_conv]
        .astype(jnp.bfloat16)
        .reshape(row_count, heads_here, VALUE_DIM)
    )
    conv_gate = rounded(projected[:, offset_conv : offset_conv + channels])
    conv_left = rounded(projected[:, offset_conv + channels : offset_conv + 2 * channels])
    conv_right = rounded(projected[:, offset_conv + 2 * channels : offset_gate])
    in_pre = projected[:, offset_gate : offset_gate + heads_here]
    forget_pre = projected[:, offset_gate + heads_here : offset_gate + 2 * heads_here] + bias_here
    log_forget = jax.nn.log_sigmoid(forget_pre) + forget_extra
    cumulative = jnp.cumsum(log_forget, axis=0)
    decay_total = cumulative[row_count - 1]
    weight_log = decay_total[None, :] - cumulative + in_pre
    block_max = jnp.max(weight_log, axis=0)
    keyed = key_rows.astype(jnp.float32) * jnp.exp(weight_log - block_max[None, :])[:, :, None]
    block_norm = jnp.sum(keyed, axis=0)
    block_memory = jnp.einsum(
        "shd,shv->hdv", keyed.astype(jnp.bfloat16), value_rows, preferred_element_type=jnp.float32
    )
    product = (conv_left * conv_right).astype(jnp.bfloat16)
    edge_rows = product[row_count - (TAPS - 1) :]
    before_rows = from_behind(edge_rows, SP, 1)
    prior_decay, prior_max, prior_memory, prior_norm = entering(
        (decay_total, block_max, block_memory, block_norm),
        SP,
        join_states,
        (
            jnp.zeros_like(decay_total),
            jnp.full_like(block_max, very_negative),
            jnp.zeros_like(block_memory),
            jnp.zeros_like(block_norm),
        ),
    )
    enter_max = jnp.maximum(prior_max, prior_decay)
    from_prior = jnp.exp(prior_max - enter_max)
    from_first = jnp.exp(prior_decay - enter_max)
    carry_memory = (
        from_prior[:, None, None] * prior_memory + from_first[:, None, None] * first_memory
    )
    carry_norm = from_prior[:, None] * prior_norm + from_first[:, None] * first_norm
    query_scale = KEY_DIM ** (-0.5)
    row_ids = lax.iota(jnp.int32, row_count)
    causal = row_ids[:, None] >= row_ids[None, :]
    cum_heads = cumulative.T
    log_gap = cum_heads[:, :, None] - cum_heads[:, None, :] + in_pre.T[:, None, :]
    log_gap = jnp.where(causal[None], log_gap, -jnp.inf)
    inter_log = cum_heads + enter_max[:, None]
    row_max = jnp.maximum(inter_log, jnp.max(log_gap, axis=2))
    raw_scores = (
        jnp.einsum("thd,shd->hts", query_rows, key_rows, preferred_element_type=jnp.float32)
        * query_scale
    )
    mixing = raw_scores * jnp.exp(log_gap - row_max[:, :, None])
    carried = jnp.exp(inter_log - row_max).T
    scaled_query = query_rows.astype(jnp.float32) * query_scale
    from_values = jnp.einsum(
        "hts,shv->thv", mixing.astype(jnp.bfloat16), value_rows, preferred_element_type=jnp.float32
    )
    from_memory = jnp.einsum("thd,hdv->thv", scaled_query, carry_memory, precision=highest)
    from_norm = jnp.einsum("thd,hd->th", scaled_query, carry_norm, precision=highest)
    numerator = from_values + carried[:, :, None] * from_memory
    denominator = jnp.sum(mixing, axis=2).T + carried * from_norm
    memory_out = numerator / jnp.maximum(jnp.abs(denominator), 1.0)[:, :, None]
    local_squares = jnp.sum(memory_out * memory_out, axis=(1, 2))
    row_total = lax.psum(local_squares, "tp")
    row_scale = lax.rsqrt(row_total / V_WIDTH + epsilon)
    heads_out = memory_out * row_scale[:, None, None]
    heads_out = heads_out.reshape(row_count, value_width).astype(jnp.bfloat16)
    padded = jnp.concatenate([before_rows, product], axis=0).astype(jnp.float32)
    filtered = taps_here[0][None, :] * padded[0:row_count]
    for tap_index in range(1, TAPS):
        filtered = (
            filtered + taps_here[tap_index][None, :] * padded[tap_index : tap_index + row_count]
        )
    conv_branch = (conv_gate * filtered).astype(jnp.bfloat16)
    return lax.psum_scatter(
        (
            jnp.dot(heads_out, w_out_memory, preferred_element_type=jnp.float32)
            + jnp.dot(conv_branch, w_out_conv, preferred_element_type=jnp.float32)
        ).astype(jnp.bfloat16),
        "tp",
        scatter_dimension=0,
        tiled=True,
    )


def solution(mesh):
    split = Mesh(mesh.devices.reshape(8, 4, mesh.shape["tp"]), ("sp_0", "sp_1", "tp"))
    placed = (
        P(SP_TP, None),
        P(),
        P(None, "tp"),
        P(None, "tp"),
        P(None, "tp"),
        P(),
        P(),
        P(),
        P(SP, "tp"),
        P(None, "tp"),
        P(None, "tp"),
        P(None, "tp"),
        P(),
        P("tp", None, None),
        P("tp", None),
        P("tp", None),
        P("tp", None),
    )
    return jax.shard_map(
        per_device, mesh=split, in_specs=placed, out_specs=P(SP_TP, None), check_vma=False
    )
```

profile of v0, /device:TPU:1, one launch (start us, length us, event | category | flops | bytes accessed | tf_op | source)
XLA Modules:
  0.0 205.7 jit_solution(9044216374947095805)
XLA Ops:
  6.5 1.3 fusion.4
  7.8 1.9 fusion.6
  9.7 0.0 all-gather.7.cloned.1.call-update
  9.8 0.0 all-gather.9.cloned.1.call-start
  9.8 1.2 dynamic_slice.13
  11.0 0.9 constant_dynamic-slice_fusion
  11.9 32.5 %all-gather.7.cloned.1.call-done = bf16[768,2048]{1,0:T(8,128)(2,1)} async-done(((bf16[96,2048]{1,0:T(8,128)(2,1)}), bf16[768,2048]{1,0:T(8,128)(2,1)}) %all-gather.7.cloned.1.call-update) | async-done | bytes 3145744 | tf_op jit(solution)/shard_map/all_gather | solution.py:113
  44.4 2.8 %convolution_reduce_fusion.1 = f32[768]{0:T(1024)S(1)} fusion(bf16[768,2048]{1,0:T(8,128)(2,1)} %all-gather.7.cloned.1.call-done, bf16[2048,8]{0,1:T(8,128)(2,1)} %param.23, s32[]{:T(128)S(6)} %select_n.346), kind=kOutput, calls=%fused_computation.18 | convolution fusion | flops 3145728 | bytes 3156996 | tf_op jit(solution)/shard_map/dot_general | solution.py:115
  47.2 0.6 fusion.118
  47.8 0.3 reduce-window.6
  48.1 0.2 slice_reduce_fusion
  48.3 0.2 reduce-window.9
  48.4 0.6 slice.336
  49.0 0.1 broadcast_bitcast_fusion
  49.1 0.6 slice.337
  50.9 0.0 copy-start.9
  50.9 3.0 %convolution_reduce_fusion = f32[768]{0:T(1024)S(1)} fusion(bf16[768,2048]{1,0:T(8,128)(2,1)} %all-gather.7.cloned.1.call-done, bf16[2048,8]{0,1:T(8,128)(2,1)} %param.22, s32[]{:T(128)S(6)} %select_n.346), kind=kOutput, calls=%fused_computation.17 | convolution fusion | flops 3145728 | bytes 3156996 | tf_op jit(solution)/shard_map/dot_general | solution.py:115
  53.9 0.6 fusion.119
  54.5 0.5 pad.22
  55.1 0.5 subtract_exponential_fusion.1
  55.6 0.0 copy-start.6
  55.7 1.0 fusion.19
  56.7 0.2 copy-done.6
  56.9 1.0 convolution_convert_fusion.3
  57.9 0.4 fusion.21
  58.3 11.1 %all-gather.2 = f32[4,131,256]{2,1,0:T(8,128)S(1)} all-gather(f32[1,131,256]{2,1,0:T(8,128)S(1)} %maximum_bitcast_fusion), channel_id=2, replica_groups=mesh['sp_0'=8,'sp_1'=4,'tp'=8] {'sp_1'}, dimensions={0}, use_global_device_ids=true | all-gather | bytes 670720 | tf_op jit(solution)/shard_map/all_gather | solution.py:40
  69.4 0.6 fusion.192
  70.0 0.6 fusion.193
  81.3 0.1 fusion.216
  81.4 0.7 maximum_bitcast_fusion.1
  82.0 0.0 all-gather.9.cloned.1.call-update
  82.1 0.0 reduce-scatter.2.cloned.1.call-start
  82.1 0.0 copy-start.7
  82.1 3.3 %convolution_convert_fusion = bf16[768,256]{1,0:T(8,128)(2,1)S(1)} fusion(bf16[768,2048]{1,0:T(8,128)(2,1)} %all-gather.7.cloned.1.call-done, bf16[2048,256]{1,0:T(8,128)(2,1)} %param.28), kind=kOutput, calls=%fused_computation.10 | convolution fusion | flops 805502976 | bytes 4587520 | tf_op jit(solution)/shard_map/dot_general | solution.py:115
  85.5 0.1 copy-done.7
  85.6 1.0 convolution_convert_fusion.1
  86.5 0.1 multiply_convert_fusion
  86.7 0.0 copy-start.8
  86.7 2.4 %collective-permute-start = (bf16[2,256]{1,0:T(2,128)(2,1)S(1)}, bf16[2,256]{1,0:T(2,128)(2,1)S(1)}, u32[]{:S(2)}, u32[]{:S(2)}) collective-permute-start(bf16[2,256]{1,0:T(2,128)(2,1)S(1)} %slice.392), channel_id=1, source_target_pairs={{0,8},{8,16},{16,24},{24,32},{32,40},{40,48},{48,56},{56,64},{64,7... | collective-permute-start | bytes 3080 | tf_op jit(solution)/shard_map/ppermute | solution.py:23
  89.1 1.0 convolution_convert_fusion.5
  90.1 1.7 convolution_convert_fusion.2
  91.8 0.3 select_reduce_fusion
  92.9 0.0 collective-permute-done
  92.9 0.1 maximum_convert_fusion
  93.0 24.6 %all-gather.9.cloned.1.call-done = f32[8,131,256]{2,1,0:T(8,128)} async-done(((f32[1,131,256]{2,1,0:T(8,128)}), f32[8,131,256]{2,1,0:T(8,128)}) %all-gather.9.cloned.1.call-update) | async-done | bytes 1073168 | tf_op jit(solution)/shard_map/all_gather | solution.py:40
  117.6 1.0 fusion.188
  118.6 0.6 fusion.190
  119.2 0.6 fusion.191
  140.9 0.7 fusion.194
  141.6 0.0 copy-start.12
  141.7 0.0 copy-start.11
  141.7 0.5 convolution_bitcast_fusion
  142.2 0.1 copy-done.12
  142.3 0.5 convolution_reduce_fusion.2
  142.8 2.5 %multiply_reduce_fusion = (f32[768]{0:T(1024)S(1)}, f32[1,256,768]{2,1,0:T(8,128)S(1)}) fusion(f32[768]{0:T(1024)S(1)} %get-tuple-element.5, f32[1,256,768]{2,1,0:T(8,128)S(1)} %convolution_bitcast_fusion, bf16[768,128]{1,0:T(8,128)(2,1)S(1)} %convolution_convert_fusion.5, f32[8,131,256]{2,1,0:T(8,128)} %all-gather.9.cloned.1.call-done, ...), kind=kOutput, calls=%fused_computation.34 | convolution fusion | flops 305200384 | bytes 3902464 | tf_op jit(solution)/shard_map/thd,hdv->thv/dot_general | solution.py:199
  145.3 17.2 %psum.7 = f32[768]{0:T(1024)S(1)} all-reduce(f32[768]{0:T(1024)S(1)} %get-tuple-element.48), channel_id=1, replica_groups=mesh['sp_0'=8,'sp_1'=4,'tp'=8] {'tp'}, use_global_device_ids=true, to_apply=%region_8.9 | all-reduce | flops 768 | bytes 6144 | tf_op jit(solution)/shard_map/psum | solution.py:205
  162.5 0.0 copy-start.3
  162.5 0.0 copy-start.4
  162.5 1.0 fusion.12
  163.5 0.2 copy-done.3
  163.7 0.1 copy-done.4
  163.8 2.9 %add_convert_fusion = bf16[768,2048]{1,0:T(8,128)(2,1)} fusion(f32[768,2048]{1,0:T(8,128)S(1)} %fusion.12, bf16[256,2048]{1,0:T(8,128)(2,1)S(1)} %copy-done.3, f32[770,256]{1,0:T(8,128)S(1)} %maximum_convert_fusion, bf16[768,256]{1,0:T(8,128)(2,1)S(1)} %copy-done.4, f32[256]{0:T(256)S(1)} %bitcast.178, f32[256]{0:T(256)S(1)} %bitcast.177, f32[256]{0:T(256)S(1)} %bitcast.176), kind=kOutput, calls=%fused_computation | convolution fusion | flops 810024960 | bytes 13241344 | tf_op jit(solution)/shard_map/dot_general | solution.py:219
  166.6 0.0 reduce-scatter.2.cloned.1.call-update
  166.7 32.5 %reduce-scatter.2.cloned.1.call-done = bf16[96,2048]{1,0:T(8,128)(2,1)} async-done(((bf16[768,2048]{1,0:T(8,128)(2,1)}), bf16[96,2048]{1,0:T(8,128)(2,1)}) %reduce-scatter.2.cloned.1.call-update) | async-done | bytes 393232 | tf_op jit(solution)/shard_map/reduce_scatter | solution.py:216
  (36 shorter events, 0.2 us)
Async XLA Ops:
  6.5 155.9 %copy-start = (bf16[256,2048]{1,0:T(8,128)(2,1)S(1)}, bf16[256,2048]{1,0:T(8,128)(2,1)}, u32[]{:S(2)}) copy-start(bf16[256,2048]{1,0:T(8,128)(2,1)} %param.32) | copy-start | bytes 3145732
  6.5 37.8 %all-gather.7.cloned.1.call-start = ((), (), s32[]{:S(2)}) async-start(), calls=%async_computation.1 | async-start | bytes 3538944 | tf_op jit(solution)/shard_map/all_gather | solution.py:113
  9.8 107.9 %all-gather.9.cloned.1.call-start = ((), (), s32[]{:S(2)}) async-start(), calls=%async_computation.3 | async-start | bytes 1253376 | tf_op jit(solution)/shard_map/all_gather | solution.py:40
  11.9 35.8 %copy-start.5 = (f32[768,1]{0,1:T(1,128)S(1)}, f32[768,1]{0,1:T(1,128)}, u32[]{:S(2)}) copy-start(f32[768,1]{0,1:T(1,128)} %param.25) | copy-start | bytes 9220
  50.9 4.8 %copy-start.1 = (bf16[768,2048]{1,0:T(8,128)(2,1)S(1)}, bf16[768,2048]{1,0:T(8,128)(2,1)}, u32[]{:S(2)}) copy-start(bf16[768,2048]{1,0:T(8,128)(2,1)} %all-gather.7.cloned.1.call-done) | copy-start | bytes 9437188
  50.9 4.8 %copy-start.9 = (bf16[2048,128]{1,0:T(8,128)(2,1)S(1)}, bf16[2048,128]{1,0:T(8,128)(2,1)}, u32[]{:S(2)}) copy-start(bf16[2048,128]{1,0:T(8,128)(2,1)} %param.20) | copy-start | bytes 1572868
  55.6 1.2 copy-start.6
  82.1 117.1 %reduce-scatter.2.cloned.1.call-start = ((), (), s32[]{:S(2)}) async-start(), calls=%async_computation.2 | async-start | bytes 3538944 | tf_op jit(solution)/shard_map/reduce_scatter | solution.py:216
  82.1 3.3 %copy-start.2 = (bf16[768,2048]{1,0:T(8,128)(2,1)S(1)}, bf16[768,2048]{1,0:T(8,128)(2,1)}, u32[]{:S(2)}) copy-start(bf16[768,2048]{1,0:T(8,128)(2,1)} %all-gather.7.cloned.1.call-done) | copy-start | bytes 9437188
  82.1 3.4 %copy-start.7 = (bf16[2048,256]{1,0:T(8,128)(2,1)S(1)}, bf16[2048,256]{1,0:T(8,128)(2,1)}, u32[]{:S(2)}) copy-start(bf16[2048,256]{1,0:T(8,128)(2,1)} %param.27) | copy-start | bytes 3145732
  85.5 3.5 %copy-start.10 = (bf16[2048,128]{1,0:T(8,128)(2,1)S(1)}, bf16[2048,128]{1,0:T(8,128)(2,1)}, u32[]{:S(2)}) copy-start(bf16[2048,128]{1,0:T(8,128)(2,1)} %param.19) | copy-start | bytes 1572868
  86.7 3.4 %copy-start.8 = (bf16[2048,256]{1,0:T(8,128)(2,1)S(1)}, bf16[2048,256]{1,0:T(8,128)(2,1)}, u32[]{:S(2)}) copy-start(bf16[2048,256]{1,0:T(8,128)(2,1)} %param.26) | copy-start | bytes 3145732
  86.7 6.2 %collective-permute-start = (bf16[2,256]{1,0:T(2,128)(2,1)S(1)}, bf16[2,256]{1,0:T(2,128)(2,1)S(1)}, u32[]{:S(2)}, u32[]{:S(2)}) collective-permute-start(bf16[2,256]{1,0:T(2,128)(2,1)S(1)} %slice.392), channel_id=1, source_target_pairs={{0,8},{8,16},{16,24},{24,32},{32,40},{40,48},{48,56},{56,64},{64,7... | collective-permute-start | bytes 3080 | tf_op jit(solution)/shard_map/ppermute | solution.py:23
  141.6 0.7 copy-start.12
  141.7 1.1 copy-start.11
  162.5 1.2 copy-start.3
  162.5 1.3 copy-start.4
Sparse Core Ops, SparseCore 0:
  9.9 34.4 all-gather.6
  82.2 35.3 all-gather.8
  166.8 32.3 reduce-scatter.1
where the time goes:
time: 208 us; the launch traced here: 206 us
  waiting for transfers between devices  89.7 us (43%)
  between operations  47.3 us (23%)
  blocking collectives  28.3 us (14%)
  matrix products  23.2 us (11%)
  local copies, waits for them, and re-layouts  8.19 us (4%)
  other arithmetic  6.7 us (3%)
  starting transfers between devices  2.46 us (1%)
    reduce_scatter x1, waiting for transfers between devices, per_device(): lax.psum_scatter((jnp.dot(heads_out, w_out_memory, preferred_element_type...  32.5 us
    all_gather x1, waiting for transfers between devices, per_device(): sub_rows = lax.all_gather(normed, 'tp', axis=0, tiled=True)  32.5 us
    all_gather x1, waiting for transfers between devices, collected_together(): both, at, found = (lax.all_gather(jnp.concatenate(lines), axis), 0, {})  24.6 us
    psum x1, blocking collectives, per_device(): row_total = lax.psum(local_squares, 'tp')  17.2 us
    dot_general x8, matrix products, per_device(): jnp.dot(sub_rows, weight, preferred_element_type=jnp.float32)  14.8 us
    all_gather x1, blocking collectives, collected_together(): both, at, found = (lax.all_gather(jnp.concatenate(lines), axis), 0, {})  11.1 us
  transfers between devices with their start and end apart: 4, of which 3 were waited for; matrix products, arithmetic and copies ran while one was open for 5% of the time, Pallas kernels for 0%

commit v1 on v0

v1 whole, which is shorter than its diff:
```python
import functools

import jax
import jax.numpy as jnp
from jax import lax
from jax.experimental import pallas as pl
from jax.experimental.pallas import tpu as pltpu
from jax.sharding import PartitionSpec as P

D = 2048
KEY = 128
VAL = 256
CH = 256
ROWS = 96
HALF = 48
BLK = 768
NTP = 8
TILES = 32
COLS = 1024
EPS = 1e-06
SCALE = KEY ** (-0.5)
MESH = pl.DeviceIdType.MESH
f32 = jnp.float32
bf16 = jnp.bfloat16


def nt_dot(a, b):
    return lax.dot_general(a, b, (((1,), (1,)), ((), ())), preferred_element_type=f32)


def tn_dot(a, b):
    return lax.dot_general(a, b, (((0,), (0,)), ((), ())), preferred_element_type=f32)


def dot(a, b):
    return jnp.dot(a, b, preferred_element_type=f32)


def kernel(
    n_sp,
    tok, gain, wi, wf, bias, fextra, taps, fmem, fnorm,
    wq, wk, wv, wcg, wcl, wcr, wom, woc,
    out,
    x, w_all, wg, wom_v, woc_v,
    proj, gates, urow, cmcol, st, rv, aux, cv, cr, mh, nh, cmem, pv, rs,
    mob, cbr, prod, eb, er, ss, scol,
    pb_c, x_c, fs_c, fr_c, gs_c, gr_c,
    pb_h, x_h, fs_h, fr_h, gs_h, gr_h,
    wsem, ag_s, ag_r, aux_s, aux_r, st_s, st_r, cr_s, cr_r, ed_s, ed_r, ss_s, ss_r,
    rc_s, rc_r, rh_s, rh_r,
):
    tpd = TILES // n_sp
    sp = lax.axis_index("sp")
    me = lax.axis_index("tp")
    y = me // 2
    c = lax.rem(me, 2)
    sib = me + 1 - 2 * c
    yn_y, yp_y, yo_y = lax.rem(y + 1, 4), lax.rem(y + 3, 4), lax.rem(y + 2, 4)
    yn, yp, yo = yn_y * 2 + c, yp_y * 2 + c, yo_y * 2 + c

    def to(peer):
        return (sp, peer)

    def sp_peer(k):
        return lax.rem(sp + k, n_sp)

    weights = [
        pltpu.make_async_copy(src, dst, wsem.at[i])
        for i, (src, dst) in enumerate(
            [
                (wk, w_all.at[:, pl.ds(0, 128)]),
                (wq, w_all.at[:, pl.ds(128, 128)]),
                (wv, w_all.at[:, pl.ds(256, 256)]),
                (wcl, w_all.at[:, pl.ds(512, 256)]),
                (wcr, w_all.at[:, pl.ds(768, 256)]),
                (wcg, w_all.at[:, pl.ds(1024, 256)]),
                (woc, woc_v),
                (wom, wom_v),
            ]
        )
    ]
    barrier = pltpu.get_barrier_semaphore()
    for k in range(1, NTP):
        pl.semaphore_signal(
            barrier, inc=1, device_id=(sp, lax.rem(me + k, NTP)), device_id_type=MESH
        )

    def greet(k, _):
        pl.semaphore_signal(barrier, inc=1, device_id=(sp_peer(k), me), device_id_type=MESH)
        return 0

    lax.fori_loop(1, n_sp, greet, 0)
    for w in weights:
        w.start()

    def block(idx, h, n):
        return x.at[pl.ds(pl.multiple_of(idx * ROWS + h * HALF, 16), n), :]

    t = tok[...].astype(f32)
    scale = lax.rsqrt(jnp.mean(t * t, axis=1, keepdims=True) + EPS)
    x[pl.ds(pl.multiple_of(me * ROWS, 16), ROWS), :] = (t * scale * gain[...]).astype(bf16)
    pl.semaphore_wait(barrier, NTP - 1 + n_sp - 1)

    sends = []

    def send(src, dst, ssem, rsem, peer):
        cp = pltpu.make_async_remote_copy(
            src_ref=src, dst_ref=dst, send_sem=ssem, recv_sem=rsem,
            device_id=to(peer), device_id_type=MESH,
        )
        cp.start()
        sends.append(cp)

    def got(dst, rsem):
        pltpu.make_async_remote_copy(
            src_ref=dst, dst_ref=dst, send_sem=rsem, recv_sem=rsem,
            device_id=to(sib), device_id_type=MESH,
        ).wait_recv()

    def ag(idx, h, n, k, peer):
        ref = block(idx, h, n)
        send(ref, ref, ag_s.at[k], ag_r.at[k], peer)

    ag(me, 0, HALF, 0, yn)
    ag(me, 1, HALF, 3, yp)
    ag(me, 1, HALF, 1, yn)
    ag(me, 0, HALF, 4, yp)
    ag(me, 0, ROWS, 6, sib)

    gw = jnp.concatenate(
        [wi[...].astype(f32), wf[...].astype(f32), jnp.zeros((112, D), f32)], axis=0
    )
    wg[...] = gw.T.astype(bf16)
    for i in range(6):
        weights[i].wait()

    def project(yy, lo, hi, with_gates):
        rows = pl.ds(pl.multiple_of(yy * 192, 64), 192)

        def step(i, _):
            cols = pl.ds(pl.multiple_of(i * 256, 256), 256)
            proj[rows, cols] = dot(x[rows, :], w_all[:, cols]).astype(bf16)
            return 0

        if with_gates:
            gates[rows, :] = dot(x[rows, :], wg[...])
        lax.fori_loop(lo, hi, step, 0)

    other = 1 - c
    got(block(sib, 0, ROWS), ag_r.at[6])
    project(y, 0, 5, True)
    got(block(yp, 0, HALF), ag_r.at[0])
    ag(yp, 0, HALF, 2, yn)
    ag(yp, 0, HALF, 7, sib)
    got(block(yn, 1, HALF), ag_r.at[3])
    ag(yn, 1, HALF, 5, yp)
    ag(yn, 1, HALF, 9, sib)
    got(block(yp, 1, HALF), ag_r.at[1])
    ag(yp, 1, HALF, 8, sib)
    got(block(yn, 0, HALF), ag_r.at[4])
    ag(yn, 0, HALF, 10, sib)
    got(block(yp_y * 2 + other, 0, HALF), ag_r.at[7])
    got(block(yp_y * 2 + other, 1, HALF), ag_r.at[8])
    project(yp_y, 0, 5, True)
    got(block(yn_y * 2 + other, 1, HALF), ag_r.at[9])
    got(block(yn_y * 2 + other, 0, HALF), ag_r.at[10])
    project(yn_y, 0, 5, True)
    got(block(yo, 0, HALF), ag_r.at[2])
    ag(yo, 0, HALF, 11, sib)
    got(block(yo, 1, HALF), ag_r.at[5])
    ag(yo, 1, HALF, 12, sib)
    got(block(yo_y * 2 + other, 0, HALF), ag_r.at[11])
    got(block(yo_y * 2 + other, 1, HALF), ag_r.at[12])
    project(yo_y, 0, 2, True)

    g_t = gates[...].T
    sub = lax.broadcasted_iota(jnp.int32, (8, BLK), 0)
    lane = lax.broadcasted_iota(jnp.int32, (8, BLK), 1)
    in_row = jnp.sum(jnp.where(sub == me, g_t[0:8], 0.0), axis=0, keepdims=True)
    f_row = jnp.sum(jnp.where(sub == me, g_t[8:16], 0.0), axis=0, keepdims=True)
    f_row = f_row + bias[me]
    log_forget = jnp.minimum(f_row, 0.0) - jnp.log1p(jnp.exp(-jnp.abs(f_row))) + fextra[...]
    cum = jnp.broadcast_to(log_forget, (8, BLK))
    for s in (1, 2, 4, 8, 16, 32, 64, 128, 256, 512):
        cum = cum + jnp.where(lane >= s, pltpu.roll(cum, s, 1), 0.0)
    u = in_row - cum
    top = u
    for s in (1, 2, 4, 8, 16, 32, 64, 128, 256, 512):
        top = jnp.maximum(top, jnp.where(lane >= s, pltpu.roll(top, s, 1), -jnp.inf))
    u_max = jnp.max(u, axis=1, keepdims=True)
    decay = jnp.sum(jnp.where(lane == BLK - 1, cum, 0.0), axis=1, keepdims=True)
    ew = jnp.exp(u - u_max)
    urow[...] = u
    cols = jnp.concatenate(
        [jnp.where(sub == 0, top, ew), jnp.zeros((120, BLK), f32)], axis=0
    ).T
    cmcol[...] = jnp.broadcast_to(cols[:, 0:1], (BLK, 128))
    keyed = proj[:, 0:128].astype(f32) * cols[:, 1:2]
    block_norm = jnp.sum(keyed, axis=0, keepdims=True)
    mem = tn_dot(keyed.astype(bf16), proj[:, 256:512])
    for p in range(TILES):
        i, j = p // 2, p % 2
        st[p // tpd, p % tpd] = mem[8 * i : 8 * i + 8, 128 * j : 128 * j + 128]
    d_lanes = jnp.broadcast_to(decay[0:1], (1, 128))
    m_lanes = jnp.broadcast_to(decay[0:1] + u_max[0:1], (1, 128))
    aux[sp] = jnp.concatenate([d_lanes, m_lanes, block_norm], axis=1)

    def state_copies(k):
        p = sp_peer(k)
        one = pltpu.make_async_remote_copy(
            src_ref=aux.at[sp], dst_ref=aux.at[sp], send_sem=aux_s, recv_sem=aux_r,
            device_id=(p, me), device_id_type=MESH,
        )
        two = pltpu.make_async_remote_copy(
            src_ref=st.at[p], dst_ref=rv.at[sp], send_sem=st_s, recv_sem=st_r,
            device_id=(p, me), device_id_type=MESH,
        )
        return one, two

    def send_state(k, _):
        for cp in state_copies(k):
            cp.start()
        return 0

    lax.fori_loop(1, n_sp, send_state, 0)
    rv[sp] = st[sp]

    project(yo_y, 2, 5, False)
    product = (proj[:, 512:768].astype(f32) * proj[:, 768:1024].astype(f32)).astype(bf16)
    eb[...] = product[BLK - 16 :]
    nxt = lax.rem(sp + 1, n_sp)
    edge = pltpu.make_async_remote_copy(
        src_ref=eb, dst_ref=er, send_sem=ed_s, recv_sem=ed_r,
        device_id=(nxt, me), device_id_type=MESH,
    )
    edge.start()
    prod[8:, :] = product.astype(f32)
    edge.wait_recv()
    prod[0:8, :] = jnp.where(sp > 0, er[...].astype(f32)[8:16], 0.0)
    mine = pl.ds(pl.multiple_of(me * CH, CH), CH)
    filtered = taps[0:1, mine] * prod[6 : 6 + BLK, :]
    filtered = filtered + taps[1:2, mine] * prod[7 : 7 + BLK, :]
    filtered = filtered + taps[2:3, mine] * prod[8 : 8 + BLK, :]
    cbr[...] = (proj[:, 1024:1280].astype(f32) * filtered).astype(bf16)

    def own(d):
        return pl.ds(pl.multiple_of((d * 2 + c) * ROWS, 16), ROWS)

    def his(d):
        return pl.ds(pl.multiple_of((d * 2 + 1 - c) * ROWS, 16), ROWS)

    def rs_start(a, wv_, pb, xb, fs, fr, gs, gr, s_, r_):
        for n, d in ((0, yo_y), (1, yn_y), (2, yp_y), (3, y)):
            rows = pl.ds(pl.multiple_of(d * 192, 64), 192)

            def step(i, _, rows=rows):
                cs = pl.ds(pl.multiple_of(i * 512, 512), 512)
                pb[rows, cs] = dot(a[rows, :], wv_[:, cs]).astype(bf16)
                return 0

            lax.fori_loop(0, 4, step, 0)
            send(pb.at[his(d)], xb.at[d], s_.at[n], r_.at[n], sib)
            if n == 1:
                got(xb.at[yo_y], r_.at[0])
                tot = pb[own(yo_y), :].astype(f32) + xb[yo_y].astype(f32)
                fs[0] = tot[:, :COLS].astype(bf16)
                fs[1] = tot[:, COLS:].astype(bf16)
                send(fs.at[0], fr.at[0], s_.at[4], r_.at[4], yn)
                send(fs.at[1], fr.at[1], s_.at[5], r_.at[5], yp)
        got(xb.at[yn_y], r_.at[1])
        tot = pb[own(yn_y), COLS:].astype(f32) + xb[yn_y, :, COLS:].astype(f32)
        gs[1] = tot.astype(bf16)
        send(gs.at[1], gr.at[1], s_.at[7], r_.at[7], yn)
        got(xb.at[yp_y], r_.at[2])
        tot = pb[own(yp_y), :COLS].astype(f32) + xb[yp_y, :, :COLS].astype(f32)
        gs[2] = tot.astype(bf16)
        send(gs.at[2], gr.at[2], s_.at[8], r_.at[8], yp)

    def rs_mid(a, wv_, pb, xb, fs, fr, gs, gr, s_, r_):
        got(fr.at[0], r_.at[4])
        tot = pb[own(yn_y), :COLS].astype(f32) + xb[yn_y, :, :COLS].astype(f32)
        gs[0] = (tot + fr[0].astype(f32)).astype(bf16)
        send(gs.at[0], gr.at[0], s_.at[6], r_.at[6], yn)
        got(fr.at[1], r_.at[5])
        tot = pb[own(yp_y), COLS:].astype(f32) + xb[yp_y, :, COLS:].astype(f32)
        gs[3] = (tot + fr[1].astype(f32)).astype(bf16)
        send(gs.at[3], gr.at[3], s_.at[9], r_.at[9], yp)

    def rs_end(a, wv_, pb, xb, fs, fr, gs, gr, s_, r_):
        got(xb.at[y], r_.at[3])
        for k in range(4):
            got(gr.at[k], r_.at[6 + k])

        def half(k):
            cs = pl.ds(k * COLS, COLS)
            own_sum = pb[own(y), cs].astype(f32) + xb[y, :, cs].astype(f32)
            return own_sum + gr[k].astype(f32) + gr[2 + k].astype(f32)

        return half

    conv_set = (cbr, woc_v, pb_c, x_c, fs_c, fr_c, gs_c, gr_c, rc_s, rc_r)
    head_set = (mob, wom_v, pb_h, x_h, fs_h, fr_h, gs_h, gr_h, rh_s, rh_r)
    weights[6].wait()
    weights[7].wait()
    rs_start(*conv_set)

    for rb in range(3):
        r0 = rb * 256
        q = proj[r0 : r0 + 256, 128:256]
        cm = cmcol[r0 : r0 + 256, 0:1]
        acc = jnp.zeros((256, VAL), f32)
        tot = jnp.zeros((256, 1), f32)
        for cb in range(rb + 1):
            c0 = cb * 256
            mix = nt_dot(q, proj[c0 : c0 + 256, 0:128]) * SCALE
            mix = mix * jnp.exp(urow[0:1, c0 : c0 + 256] - cm)
            if cb == rb:
                ri = lax.broadcasted_iota(jnp.int32, (256, 256), 0)
                ci = lax.broadcasted_iota(jnp.int32, (256, 256), 1)
                mix = jnp.where(ri >= ci, mix, 0.0)
            tot = tot + jnp.sum(mix, axis=1, keepdims=True)
            acc = acc + dot(mix.astype(bf16), proj[c0 : c0 + 256, 256:512])
        pv[r0 : r0 + 256, :] = acc
        rs[r0 : r0 + 256, :] = jnp.broadcast_to(tot, (256, 128))

    rest = pl.ds(0, n_sp - 1)
    got(aux.at[rest], aux_r)
    got(rv.at[rest], st_r)
    first = []
    for k in range(tpd):
        p = sp * tpd + k
        r_i = pl.ds(pl.multiple_of((p // 2) * 8, 8), 8)
        c_i = pl.ds(pl.multiple_of(lax.rem(p, 2) * 128, 128), 128)
        first.append(fmem[r_i, c_i])
    run_m = jnp.zeros((1, 128), f32)
    run_n = fnorm[...]
    for b in range(n_sp):
        for k in range(tpd):
            cv[b, k] = first[k]
        mh[b] = run_m
        nh[b] = run_n
        if b < n_sp - 1:
            row = aux[b]
            new_m = jnp.maximum(run_m + row[:, 0:128], row[:, 128:256])
            old = jnp.exp(run_m + row[:, 0:128] - new_m)
            new = jnp.exp(row[:, 128:256] - new_m)
            first = [old * first[k] + new * rv[b, k] for k in range(tpd)]
            run_n = old * run_n + new * row[:, 256:384]
            run_m = new_m

    def carry_copy(k):
        p = sp_peer(k)
        return pltpu.make_async_remote_copy(
            src_ref=cv.at[p], dst_ref=cr.at[sp], send_sem=cr_s, recv_sem=cr_r,
            device_id=(p, me), device_id_type=MESH,
        )

    def send_carry(k, _):
        carry_copy(k).start()
        return 0

    lax.fori_loop(1, n_sp, send_carry, 0)
    cr[sp] = cv[sp]
    rs_mid(*conv_set)

    got(cr.at[rest], cr_r)
    for p in range(TILES):
        i, j = p // 2, p % 2
        cmem[8 * i : 8 * i + 8, 128 * j : 128 * j + 128] = cr[p // tpd, p % tpd]
    carry = cmem[...]
    high = carry.astype(bf16)
    low = (carry - high.astype(f32)).astype(bf16)
    m_in = mh[sp][:, 0:1]
    n_in = nh[sp]
    n_1 = n_in.astype(bf16).astype(f32)
    n_2 = (n_in - n_1).astype(bf16).astype(f32)
    n_3 = n_in - n_1 - n_2
    sub16 = lax.broadcasted_iota(jnp.int32, (16, 128), 0)
    n_rows = jnp.where(
        sub16 == 0, n_1, jnp.where(sub16 == 1, n_2, jnp.where(sub16 == 2, n_3, 0.0))
    ).astype(bf16)
    squares = []
    for rb in range(3):
        r0 = rb * 256
        q = proj[r0 : r0 + 256, 128:256]
        cm = cmcol[r0 : r0 + 256, 0:1]
        peak = jnp.maximum(cm, m_in)
        f_in = jnp.exp(cm - peak)
        f_carry = jnp.exp(m_in - peak)
        from_memory = (dot(q, high) + dot(q, low)) * SCALE
        from_norm = jnp.sum(nt_dot(q, n_rows), axis=1, keepdims=True) * SCALE
        num = f_in * pv[r0 : r0 + 256, :] + f_carry * from_memory
        den = f_in * rs[r0 : r0 + 256, 0:1] + f_carry * from_norm
        memory_out = num / jnp.maximum(jnp.abs(den), 1.0)
        squares.append(jnp.sum(memory_out * memory_out, axis=1, keepdims=True))
        mob[r0 : r0 + 256, :] = memory_out.astype(bf16)
    sq = jnp.broadcast_to(jnp.concatenate(squares, axis=0), (BLK, 128)).T
    ss[me] = sq[0:1]
    for k in range(1, NTP):
        peer = lax.rem(me + k, NTP)
        send(ss.at[me], ss.at[me], ss_s.at[k], ss_r.at[k], peer)
    rs_start(*head_set)
    rs_mid(*head_set)
    for k in range(1, NTP):
        got(ss.at[lax.rem(me + NTP - k, NTP)], ss_r.at[k])
    total = ss[0]
    for k in range(1, NTP):
        total = total + ss[k]
    factor = lax.rsqrt(total / (NTP * VAL) + EPS)
    scol[...] = jnp.broadcast_to(factor, (128, BLK)).T
    conv_half = rs_end(*conv_set)
    head_half = rs_end(*head_set)
    factor = scol[pl.ds(pl.multiple_of(me * ROWS, 8), ROWS), 0:1]
    for k in range(2):
        cs = slice(k * COLS, (k + 1) * COLS)
        out[:, cs] = (factor * head_half(k) + conv_half(k)).astype(bf16)

    for cp in sends:
        cp.wait_send()
    edge.wait_send()

    def sent(ref, sem):
        pltpu.make_async_remote_copy(
            src_ref=ref, dst_ref=ref, send_sem=sem, recv_sem=sem,
            device_id=to(sib), device_id_type=MESH,
        ).wait_send()

    sent(aux.at[rest], aux_s)
    sent(st.at[rest], st_s)
    sent(cv.at[rest], cr_s)


def solution(mesh):
    n_sp = mesh.shape["sp"]
    tpd = TILES // n_sp
    vmem = pl.BlockSpec(memory_space=pltpu.VMEM)
    smem = pl.BlockSpec(memory_space=pltpu.SMEM)
    hbm = pl.BlockSpec(memory_space=pl.ANY)
    dma = pltpu.SemaphoreType.DMA

    def rs_bufs():
        return [
            pltpu.VMEM((BLK, D), bf16),
            pltpu.VMEM((4, ROWS, D), bf16),
            pltpu.VMEM((2, ROWS, COLS), bf16),
            pltpu.VMEM((2, ROWS, COLS), bf16),
            pltpu.VMEM((4, ROWS, COLS), bf16),
            pltpu.VMEM((4, ROWS, COLS), bf16),
        ]

    scratch = [
        pltpu.VMEM((BLK, D), bf16),
        pltpu.VMEM((D, 1280), bf16),
        pltpu.VMEM((D, 128), bf16),
        pltpu.VMEM((VAL, D), bf16),
        pltpu.VMEM((CH, D), bf16),
        pltpu.VMEM((BLK, 1280), bf16),
        pltpu.VMEM((BLK, 128), f32),
        pltpu.VMEM((8, BLK), f32),
        pltpu.VMEM((BLK, 128), f32),
        pltpu.VMEM((n_sp, tpd, 8, 128), f32),
        pltpu.VMEM((n_sp, tpd, 8, 128), f32),
        pltpu.VMEM((n_sp, 1, 384), f32),
        pltpu.VMEM((n_sp, tpd, 8, 128), f32),
        pltpu.VMEM((n_sp, tpd, 8, 128), f32),
        pltpu.VMEM((n_sp, 1, 128), f32),
        pltpu.VMEM((n_sp, 1, 128), f32),
        pltpu.VMEM((KEY, VAL), f32),
        pltpu.VMEM((BLK, VAL), f32),
        pltpu.VMEM((BLK, 128), f32),
        pltpu.VMEM((BLK, VAL), bf16),
        pltpu.VMEM((BLK, CH), bf16),
        pltpu.VMEM((BLK + 8, CH), f32),
        pltpu.VMEM((16, CH), bf16),
        pltpu.VMEM((16, CH), bf16),
        pltpu.VMEM((NTP, 1, BLK), f32),
        pltpu.VMEM((BLK, 128), f32),
        *rs_bufs(),
        *rs_bufs(),
        dma((8,)),
        dma((13,)),
        dma((13,)),
        dma(()),
        dma(()),
        dma(()),
        dma(()),
        dma(()),
        dma(()),
        dma(()),
        dma(()),
        dma((NTP,)),
        dma((NTP,)),
        dma((10,)),
        dma((10,)),
        dma((10,)),
        dma((10,)),
    ]

    def per_device(
        tokens, in_gain, w_query, w_key, w_value, w_input_gate, w_forget_gate, forget_bias,
        forget_extra, w_conv_gate, w_conv_left, w_conv_right, conv_taps, first_memory,
        first_norm, w_out_memory, w_out_conv,
    ):
        return pl.pallas_call(
            functools.partial(kernel, n_sp),
            out_shape=jax.ShapeDtypeStruct((ROWS, D), bf16),
            in_specs=[vmem] * 4 + [smem] + [vmem] * 4 + [hbm] * 8,
            out_specs=vmem,
            scratch_shapes=scratch,
            compiler_params=pltpu.CompilerParams(
                collective_id=0, has_side_effects=True, vmem_limit_bytes=60 * 1024 * 1024
            ),
        )(
            tokens, in_gain.reshape(1, D), w_input_gate.T, w_forget_gate.T, forget_bias,
            forget_extra.reshape(1, BLK), conv_taps, first_memory.reshape(KEY, VAL), first_norm,
            w_query, w_key, w_value, w_conv_gate, w_conv_left, w_conv_right,
            w_out_memory, w_out_conv,
        )

    placed = (
        P(("sp", "tp"), None),
        P(),
        P(None, "tp"),
        P(None, "tp"),
        P(None, "tp"),
        P(),
        P(),
        P(),
        P("sp", "tp"),
        P(None, "tp"),
        P(None, "tp"),
        P(None, "tp"),
        P(),
        P("tp", None, None),
        P("tp", None),
        P("tp", None),
        P("tp", None),
    )
    return jax.shard_map(
        per_device, mesh=mesh, in_specs=placed, out_specs=P(("sp", "tp"), None), check_vma=False
    )
```

time: 208 us -> 75.1 us (0.36); the launches traced: 206 us -> 74.9 us
  waiting for transfers between devices: 89.7 us -> 0 us
  Pallas kernels: 0 us -> 73.2 us
  between operations: 47.3 us -> 0.01 us
  blocking collectives: 28.3 us -> 0 us
  matrix products: 23.2 us -> 0 us
  other arithmetic: 6.7 us -> 0 us
  local copies, waits for them, and re-layouts: 8.19 us -> 1.77 us
  starting transfers between devices: 2.46 us -> 0 us
    pallas_call x0 -> x1, Pallas kernels: none -> 73.2 us  [per_device(): pl.pallas_call(functools.partial(kernel, n_sp), out_shape=jax.ShapeDtypeS...]
    all_gather x2 -> x0, waiting for transfers between devices: 57.1 us -> none  [the longest x1 32.5 us: per_device(): sub_rows = lax.all_gather(normed, 'tp', axis=0, tiled=True)]
    reduce_scatter x1 -> x0, waiting for transfers between devices: 32.5 us -> none  [per_device(): lax.psum_scatter((jnp.dot(heads_out, w_out_memory, preferred_element_type...]
    dot_general x15 -> x0, matrix products: 23.2 us -> none  [the longest x8 14.8 us: per_device(): jnp.dot(sub_rows, weight, preferred_element_type=jnp.float32)]
    psum x1 -> x0, blocking collectives: 17.2 us -> none  [per_device(): row_total = lax.psum(local_squares, 'tp')]
    all_gather x1 -> x0, blocking collectives: 11.1 us -> none  [collected_together(): both, at, found = (lax.all_gather(jnp.concatenate(lines), axis), 0, {})]
    slice x11 -> x0, local copies, waits for them, and re-layouts: 5.57 us -> none  [the longest x4 2.4 us: entering(): running = combine(running, jax.tree.map(lambda part: part[k], pieces))]
    ppermute x1 -> x0, starting transfers between devices: 2.38 us -> none  [from_behind(): return lax.ppermute(block, axis, route)]
  transfers between devices with their start and end apart: 4 -> 0, of which waited for: 3 -> 0; matrix products, arithmetic and copies ran while one was open for 5% -> 0% of each run, Pallas kernels for 0% -> 0%
where the time goes in v1:
time: 75.1 us; the launch traced here: 74.9 us
  Pallas kernels  73.2 us (97%)
  local copies, waits for them, and re-layouts  1.77 us (2%)
    pallas_call x1, Pallas kernels, per_device(): pl.pallas_call(functools.partial(kernel, n_sp), out_shape=jax.ShapeDtypeS...  73.2 us
    unnamed x1, local copies, waits for them, and re-layouts  1.77 us

profile of v1, /device:TPU:1, one launch (start us, length us, event | category | flops | bytes accessed | tf_op | source)
XLA Modules:
  0.0 74.9 jit_solution(14948887652158426250)
XLA Ops:
  0.0 73.2 %shard_map.163 = bf16[96,2048]{1,0:T(8,128)(2,1)} custom-call(bf16[96,2048]{1,0:T(8,128)(2,1)} %tok.1, f32[1,2048]{1,0:T(1,128)} %bitcast.8, bf16[8,2048]{1,0:T(8,128)(2,1)} %bitcast.6, bf16[8,2048]{1,0:T(8,128)(2,1)} %bitcast.7, f32[8]{0:T(128)} %bias.1, f32[1,768]{1,0:T(1,128)} %bitcast.9, f32[3,2048]{1,0:T(4,128)} %taps.1, f32[128,256]{1,0:T(8,128)} %bitcast.5, ...), custom_call_target="tpu_custom_call" | custom-call | tf_op jit(solution)/shard_map/pallas_call | solution.py:504
  73.2 1.8 %copy.19 = bf16[96,2048]{1,0:T(8,128)(2,1)} copy(bf16[96,2048]{1,0:T(8,128)(2,1)} %shard_map.163) | data formatting | bytes 786432

commit v2 on v1

v2 whole, which is shorter than its diff:
```python
import functools

import jax
import jax.numpy as jnp
from jax import lax
from jax.experimental import pallas as pl
from jax.experimental.pallas import tpu as pltpu
from jax.sharding import PartitionSpec as P

D = 2048
KEY = 128
VAL = 256
CH = 256
ROWS = 96
HALF = 48
BLK = 768
NTP = 8
TILES = 32
COLS = 1024
EPS = 1e-06
SCALE = KEY ** (-0.5)
MESH = pl.DeviceIdType.MESH
f32 = jnp.float32
bf16 = jnp.bfloat16


def nt_dot(a, b):
    return lax.dot_general(a, b, (((1,), (1,)), ((), ())), preferred_element_type=f32)


def dot(a, b):
    return jnp.dot(a, b, preferred_element_type=f32)


def kernel(
    n_sp,
    tok_h, gain_h, wi_h, wf_h, bias_h, fextra_h, taps_h, fmem_h, fnorm_h,
    wq, wk, wv, wcg, wcl, wcr, wom, woc,
    out,
    tok, gain, wi, wf, bias, fextra, taps, fmem, fnorm,
    x, w_all, wom_v, woc_v,
    proj, gates, urow, cmcol, st, rv, aux, cv, cr, mh, nh, cmem, pv, rs,
    mob, cbr, prod, eb, er, ss, scol, sqcol, fin,
    pb_c, x_c, fs_c, fr_c, gs_c, gr_c,
    pb_h, x_h, fs_h, fr_h, gs_h, gr_h,
    wsem, isem, ag_s, ag_r, aux_s, aux_r, st_s, st_r, cr_s, cr_r, ed_s, ed_r, ss_s, ss_r,
    rc_s, rc_r, rh_s, rh_r,
):
    tpd = TILES // n_sp
    scope = jax.named_scope
    sp = lax.axis_index("sp")
    me = lax.axis_index("tp")
    y = me // 2
    c = lax.rem(me, 2)
    sib = me + 1 - 2 * c
    yn_y, yp_y, yo_y = lax.rem(y + 1, 4), lax.rem(y + 3, 4), lax.rem(y + 2, 4)
    yn, yp = yn_y * 2 + c, yp_y * 2 + c

    def sp_peer(k):
        return lax.rem(sp + k, n_sp)

    inputs = [
        pltpu.make_async_copy(src, dst, isem.at[i])
        for i, (src, dst) in enumerate(
            [
                (tok_h, tok), (gain_h, gain), (wi_h, wi), (wf_h, wf), (bias_h, bias),
                (fextra_h, fextra), (taps_h, taps), (fmem_h, fmem), (fnorm_h, fnorm),
            ]
        )
    ]
    weights = [
        pltpu.make_async_copy(src, dst, wsem.at[i])
        for i, (src, dst) in enumerate(
            [
                (wk, w_all.at[:, pl.ds(0, 128)]),
                (wq, w_all.at[:, pl.ds(128, 128)]),
                (wv, w_all.at[:, pl.ds(256, 256)]),
                (wcl, w_all.at[:, pl.ds(512, 256)]),
                (wcr, w_all.at[:, pl.ds(768, 256)]),
                (wcg, w_all.at[:, pl.ds(1024, 256)]),
                (woc, woc_v),
                (wom, wom_v),
            ]
        )
    ]
    for cp in inputs[:4]:
        cp.start()
    barrier = pltpu.get_barrier_semaphore()
    for k in range(1, NTP):
        pl.semaphore_signal(
            barrier, inc=1, device_id=(sp, lax.rem(me + k, NTP)), device_id_type=MESH
        )

    def greet(k, _):
        pl.semaphore_signal(barrier, inc=1, device_id=(sp_peer(k), me), device_id_type=MESH)
        return 0

    lax.fori_loop(1, n_sp, greet, 0)
    for cp in inputs[4:]:
        cp.start()
    for w in weights:
        w.start()

    def slots(s, n=1):
        return x.at[pl.ds(pl.multiple_of(s * HALF, 16), n * HALF), :]

    with scope("norm"):
        inputs[0].wait()
        inputs[1].wait()
        t = tok[...].astype(f32)
        scale = lax.rsqrt(jnp.mean(t * t, axis=1, keepdims=True) + EPS)
        x[pl.ds(pl.multiple_of(c * ROWS, 16), ROWS), :] = (t * scale * gain[...]).astype(bf16)
    with scope("w_barrier"):
        pl.semaphore_wait(barrier, NTP - 1 + n_sp - 1)

    sends = []

    def send(src, dst, ssem, rsem, peer):
        cp = pltpu.make_async_remote_copy(
            src_ref=src, dst_ref=dst, send_sem=ssem, recv_sem=rsem,
            device_id=(sp, peer), device_id_type=MESH,
        )
        cp.start()
        sends.append(cp)

    def got(dst, rsem, name="w"):
        with scope(name):
            pltpu.make_async_remote_copy(
                src_ref=dst, dst_ref=dst, send_sem=rsem, recv_sem=rsem,
                device_id=(sp, sib), device_id_type=MESH,
            ).wait_recv()

    def ag(src, dst, k, peer, n=1):
        send(slots(src, n), slots(dst, n), ag_s.at[k], ag_r.at[k], peer)

    other = 1 - c
    ag(2 * c, 4 + c, 0, yn)
    ag(2 * c + 1, 6 + c, 3, yp)
    ag(2 * c + 1, 8 + c, 1, yn)
    ag(2 * c, 10 + c, 4, yp)
    ag(2 * c, 2 * c, 6, sib, 2)

    inputs[2].wait()
    inputs[3].wait()
    gw = jnp.concatenate(
        [wi[...].astype(f32), wf[...].astype(f32), jnp.zeros((112, D), f32)], axis=0
    )
    w_all[:, 1280:1408] = gw.T.astype(bf16)
    with scope("w_weights"):
        for i in range(6):
            weights[i].wait()

    def project(stage, bases, parts):
        xs = x[stage * 192 : stage * 192 + 192, :]
        for lo, hi in parts:
            res = dot(xs, w_all[:, lo:hi])
            for k, base in enumerate(bases):
                rows = pl.ds(pl.multiple_of(base, 16), HALF)
                piece = res[k * HALF : (k + 1) * HALF]
                if hi <= 1280:
                    proj[rows, lo:hi] = piece.astype(bf16)
                else:
                    gates[rows, :] = piece[:, 1280 - lo :]
                    if lo < 1280:
                        proj[rows, lo:1280] = piece[:, : 1280 - lo].astype(bf16)

    every = ((0, 512), (512, 1024), (1024, 1408))
    got(slots(2 * other, 2), ag_r.at[6], "w_ag6")
    with scope("proj_0"):
        project(0, [y * 192 + HALF * k for k in range(4)], every)
    got(slots(4 + c), ag_r.at[0], "w_ag0")
    ag(4 + c, 12 + c, 2, yn)
    ag(4 + c, 4 + c, 7, sib)
    got(slots(6 + c), ag_r.at[3], "w_ag3")
    ag(6 + c, 14 + c, 5, yp)
    ag(6 + c, 6 + c, 8, sib)
    got(slots(4 + other), ag_r.at[7], "w_ag7")
    got(slots(6 + other), ag_r.at[8], "w_ag8")
    with scope("proj_1"):
        project(
            1,
            [yp_y * 192, yp_y * 192 + ROWS, yn_y * 192 + HALF, yn_y * 192 + ROWS + HALF],
            every,
        )
    got(slots(8 + c), ag_r.at[1], "w_ag1")
    ag(8 + c, 8 + c, 9, sib)
    got(slots(10 + c), ag_r.at[4], "w_ag4")
    ag(10 + c, 10 + c, 10, sib)
    got(slots(8 + other), ag_r.at[9], "w_ag9")
    got(slots(10 + other), ag_r.at[10], "w_ag10")
    with scope("proj_2"):
        project(
            2,
            [yp_y * 192 + HALF, yp_y * 192 + ROWS + HALF, yn_y * 192, yn_y * 192 + ROWS],
            every,
        )
    got(slots(12 + c), ag_r.at[2], "w_ag2")
    ag(12 + c, 12 + c, 11, sib)
    got(slots(14 + c), ag_r.at[5], "w_ag5")
    ag(14 + c, 14 + c, 12, sib)
    got(slots(12 + other), ag_r.at[11], "w_ag11")
    got(slots(14 + other), ag_r.at[12], "w_ag12")
    last = [yo_y * 192, yo_y * 192 + ROWS, yo_y * 192 + HALF, yo_y * 192 + ROWS + HALF]
    with scope("proj_3"):
        project(3, last, ((1280, 1408), (0, 512)))

    for cp in inputs[4:]:
        cp.wait()
    with scope("state"):
        g_t = gates[...].T
        sub = lax.broadcasted_iota(jnp.int32, (8, BLK), 0)
        lane = lax.broadcasted_iota(jnp.int32, (8, BLK), 1)
        in_row = jnp.sum(jnp.where(sub == me, g_t[0:8], 0.0), axis=0, keepdims=True)
        f_row = jnp.sum(jnp.where(sub == me, g_t[8:16], 0.0), axis=0, keepdims=True)
        lane8 = lax.broadcasted_iota(jnp.int32, (1, NTP), 1)
        f_row = f_row + jnp.sum(jnp.where(lane8 == me, bias[...], 0.0), axis=1, keepdims=True)
        log_forget = (
            jnp.minimum(f_row, 0.0) - jnp.log1p(jnp.exp(-jnp.abs(f_row))) + fextra[...]
        )

        def stacked(row):
            parts = [row[:, 128 * k : 128 * k + 128] for k in range(6)]
            return jnp.concatenate(parts + [jnp.zeros((2, 128), f32)], axis=0)

        lf6 = stacked(log_forget)
        l_1 = lf6.astype(bf16).astype(f32)
        l_2 = (lf6 - l_1).astype(bf16).astype(f32)
        l_3 = lf6 - l_1 - l_2
        upto = lax.broadcasted_iota(jnp.int32, (128, 128), 0) <= lax.broadcasted_iota(
            jnp.int32, (128, 128), 1
        )
        sums = dot(
            jnp.concatenate([l_1, l_2, l_3, jnp.zeros((8, 128), f32)], axis=0).astype(bf16),
            jnp.where(upto, 1.0, 0.0).astype(bf16),
        )
        inside = sums[0:8] + sums[8:16] + sums[16:24]
        sub8 = lax.broadcasted_iota(jnp.int32, (8, 128), 0)
        ends = jnp.broadcast_to(inside[:, 127:128], (8, 128))
        before = jnp.where(sub8 >= 1, pltpu.roll(ends, 1, 0), 0.0)
        for s in (1, 2, 4):
            before = before + jnp.where(sub8 >= s, pltpu.roll(before, s, 0), 0.0)
        cum6 = inside + before
        u6 = jnp.where(sub8 < 6, stacked(in_row) - cum6, -jnp.inf)
        u_max = jnp.max(jnp.max(u6, axis=1, keepdims=True), axis=0, keepdims=True)
        decay = cum6[5:6, 127:128]

        def unstacked(a):
            return jnp.concatenate([a[k : k + 1] for k in range(6)], axis=1)

        u_row = unstacked(u6)
        k_t = proj[:, 0:128].astype(f32).T
        keyed = k_t * jnp.exp(u_row - u_max)
        mem = dot(keyed.astype(bf16), proj[:, 256:512])
        norm_col = jnp.sum(keyed, axis=1, keepdims=True)
        block_norm = jnp.broadcast_to(norm_col, (128, 128)).T[0:1]
        d_lanes = jnp.broadcast_to(decay, (1, 128))
        m_lanes = jnp.broadcast_to(decay + u_max, (1, 128))
        aux[sp] = jnp.concatenate([d_lanes, m_lanes, block_norm], axis=1)
        for p in range(TILES):
            i, j = p // 2, p % 2
            st[p // tpd, p % tpd] = mem[8 * i : 8 * i + 8, 128 * j : 128 * j + 128]

    def over_peers(start):
        half = n_sp // 2
        start(half)

        def both(i, _):
            start(half + i)
            start(half - i)
            return 0

        lax.fori_loop(1, half, both, 0)

    def start_state(k):
        p = sp_peer(k)
        pltpu.make_async_remote_copy(
            src_ref=st.at[p], dst_ref=rv.at[sp], send_sem=st_s, recv_sem=st_r,
            device_id=(p, me), device_id_type=MESH,
        ).start()
        pltpu.make_async_remote_copy(
            src_ref=aux.at[sp], dst_ref=aux.at[sp], send_sem=aux_s, recv_sem=aux_r,
            device_id=(p, me), device_id_type=MESH,
        ).start()

    with scope("send_state"):
        over_peers(start_state)
    rv[sp] = st[sp]

    with scope("proj_lr"):
        project(3, last, ((512, 1024),))
        product = (proj[:, 512:768].astype(f32) * proj[:, 768:1024].astype(f32)).astype(bf16)
        eb[...] = product[BLK - 16 :]
        prod[8:, :] = product.astype(f32)
    edge = pltpu.make_async_remote_copy(
        src_ref=eb, dst_ref=er, send_sem=ed_s, recv_sem=ed_r,
        device_id=(sp_peer(1), me), device_id_type=MESH,
    )
    edge.start()
    with scope("proj_g"):
        project(3, last, ((1024, 1280),))

    with scope("mixing"):
        top = jnp.broadcast_to(u_row, (8, BLK))
        urow[...] = top
        for s in (1, 2, 4, 8, 16, 32, 64, 128, 256, 512):
            top = jnp.maximum(top, jnp.where(lane >= s, pltpu.roll(top, s, 1), -jnp.inf))
        cols = jnp.concatenate([top, jnp.zeros((120, BLK), f32)], axis=0).T
        cmcol[...] = jnp.broadcast_to(cols[:, 0:1], (BLK, 128))
        for rb in range(3):
            r0 = rb * 256
            q = proj[r0 : r0 + 256, 128:256]
            cm = cmcol[r0 : r0 + 256, 0:1]
            acc = jnp.zeros((256, VAL), f32)
            tot = jnp.zeros((256, 1), f32)
            for cb in range(rb + 1):
                c0 = cb * 256
                mix = nt_dot(q, proj[c0 : c0 + 256, 0:128]) * SCALE
                mix = mix * jnp.exp(urow[0:1, c0 : c0 + 256] - cm)
                if cb == rb:
                    ri = lax.broadcasted_iota(jnp.int32, (256, 256), 0)
                    ci = lax.broadcasted_iota(jnp.int32, (256, 256), 1)
                    mix = jnp.where(ri >= ci, mix, 0.0)
                tot = tot + jnp.sum(mix, axis=1, keepdims=True)
                acc = acc + dot(mix.astype(bf16), proj[c0 : c0 + 256, 256:512])
            pv[r0 : r0 + 256, :] = acc
            rs[r0 : r0 + 256, :] = jnp.broadcast_to(tot, (256, 128))

    with scope("w_edge"):
        edge.wait_recv()
    with scope("filter"):
        prod[0:8, :] = jnp.where(sp > 0, er[...].astype(f32)[8:16], 0.0)
        mine = pl.ds(pl.multiple_of(me * CH, CH), CH)
        filtered = taps[0:1, mine] * prod[6 : 6 + BLK, :]
        filtered = filtered + taps[1:2, mine] * prod[7 : 7 + BLK, :]
        filtered = filtered + taps[2:3, mine] * prod[8 : 8 + BLK, :]
        cbr[...] = (proj[:, 1024:1280].astype(f32) * filtered).astype(bf16)

    def own(d):
        return pl.ds(pl.multiple_of((d * 2 + c) * ROWS, 16), ROWS)

    def his(d):
        return pl.ds(pl.multiple_of((d * 2 + 1 - c) * ROWS, 16), ROWS)

    def rs_start(a, wv_, pb, xb, fs, fr, gs, gr, s_, r_, prepare=None):
        for n, d in ((0, yo_y), (1, yn_y), (2, yp_y), (3, y)):
            rows = pl.ds(pl.multiple_of(d * 192, 64), 192)
            if prepare is not None:
                prepare(rows)
            for lo in range(0, D, COLS):
                pb[rows, lo : lo + COLS] = dot(a[rows, :], wv_[:, lo : lo + COLS]).astype(bf16)
            send(pb.at[his(d)], xb.at[d], s_.at[n], r_.at[n], sib)
            if n == 1:
                got(xb.at[yo_y], r_.at[0], "w_x0")
                tot = pb[own(yo_y), :].astype(f32) + xb[yo_y].astype(f32)
                fs[0] = tot[:, :COLS].astype(bf16)
                fs[1] = tot[:, COLS:].astype(bf16)
                send(fs.at[0], fr.at[0], s_.at[4], r_.at[4], yn)
                send(fs.at[1], fr.at[1], s_.at[5], r_.at[5], yp)
        got(xb.at[yn_y], r_.at[1], "w_x1")
        tot = pb[own(yn_y), COLS:].astype(f32) + xb[yn_y, :, COLS:].astype(f32)
        gs[1] = tot.astype(bf16)
        send(gs.at[1], gr.at[1], s_.at[7], r_.at[7], yn)
        got(xb.at[yp_y], r_.at[2], "w_x2")
        tot = pb[own(yp_y), :COLS].astype(f32) + xb[yp_y, :, :COLS].astype(f32)
        gs[2] = tot.astype(bf16)
        send(gs.at[2], gr.at[2], s_.at[8], r_.at[8], yp)

    def rs_mid(a, wv_, pb, xb, fs, fr, gs, gr, s_, r_):
        got(fr.at[0], r_.at[4], "w_f0")
        tot = pb[own(yn_y), :COLS].astype(f32) + xb[yn_y, :, :COLS].astype(f32)
        gs[0] = (tot + fr[0].astype(f32)).astype(bf16)
        send(gs.at[0], gr.at[0], s_.at[6], r_.at[6], yn)
        got(fr.at[1], r_.at[5], "w_f1")
        tot = pb[own(yp_y), COLS:].astype(f32) + xb[yp_y, :, COLS:].astype(f32)
        gs[3] = (tot + fr[1].astype(f32)).astype(bf16)
        send(gs.at[3], gr.at[3], s_.at[9], r_.at[9], yp)

    def here(pb, xb, cs):
        return pb[own(y), cs].astype(f32) + xb[y, :, cs].astype(f32)

    conv_set = (cbr, woc_v, pb_c, x_c, fs_c, fr_c, gs_c, gr_c, rc_s, rc_r)
    head_set = (mob, wom_v, pb_h, x_h, fs_h, fr_h, gs_h, gr_h, rh_s, rh_r)
    weights[6].wait()
    weights[7].wait()
    with scope("rs_start_conv"):
        rs_start(*conv_set)

    rest = pl.ds(0, n_sp - 1)
    got(aux.at[rest], aux_r, "w_aux")
    got(rv.at[rest], st_r, "w_state")
    first = []
    for k in range(tpd):
        p = sp * tpd + k
        r_i = pl.ds(pl.multiple_of((p // 2) * 8, 8), 8)
        c_i = pl.ds(pl.multiple_of(lax.rem(p, 2) * 128, 128), 128)
        first.append(fmem[r_i, c_i])
    run_m = jnp.zeros((1, 128), f32)
    run_n = fnorm[...]
    for b in range(n_sp):
        for k in range(tpd):
            cv[b, k] = first[k]
        mh[b] = run_m
        nh[b] = run_n
        if b < n_sp - 1:
            row = aux[b]
            new_m = jnp.maximum(run_m + row[:, 0:128], row[:, 128:256])
            old = jnp.exp(run_m + row[:, 0:128] - new_m)
            new = jnp.exp(row[:, 128:256] - new_m)
            first = [old * first[k] + new * rv[b, k] for k in range(tpd)]
            run_n = old * run_n + new * row[:, 256:384]
            run_m = new_m

    def start_carry(k):
        p = sp_peer(k)
        pltpu.make_async_remote_copy(
            src_ref=cv.at[p], dst_ref=cr.at[sp], send_sem=cr_s, recv_sem=cr_r,
            device_id=(p, me), device_id_type=MESH,
        ).start()

    with scope("send_carry"):
        over_peers(start_carry)
    cr[sp] = cv[sp]
    with scope("rs_mid_conv"):
        rs_mid(*conv_set)

    got(cr.at[rest], cr_r, "w_carry")
    with scope("carry"):
        for p in range(TILES):
            i, j = p // 2, p % 2
            cmem[8 * i : 8 * i + 8, 128 * j : 128 * j + 128] = cr[p // tpd, p % tpd]
        carry = cmem[...]
        high = carry.astype(bf16)
        low = (carry - high.astype(f32)).astype(bf16)
        m_in = mh[sp][:, 0:1]
        n_in = nh[sp]
        n_1 = n_in.astype(bf16).astype(f32)
        n_2 = (n_in - n_1).astype(bf16).astype(f32)
        n_3 = n_in - n_1 - n_2
        sub16 = lax.broadcasted_iota(jnp.int32, (16, 128), 0)
        n_rows = jnp.where(
            sub16 == 0, n_1, jnp.where(sub16 == 1, n_2, jnp.where(sub16 == 2, n_3, 0.0))
        ).astype(bf16)

    def heads(rows):
        q = proj[rows, 128:256]
        cm = cmcol[rows, 0:1]
        peak = jnp.maximum(cm, m_in)
        f_in = jnp.exp(cm - peak)
        f_carry = jnp.exp(m_in - peak)
        from_memory = (dot(q, high) + dot(q, low)) * SCALE
        from_norm = jnp.sum(nt_dot(q, n_rows), axis=1, keepdims=True) * SCALE
        num = f_in * pv[rows, :] + f_carry * from_memory
        den = f_in * rs[rows, 0:1] + f_carry * from_norm
        memory_out = num / jnp.maximum(jnp.abs(den), 1.0)
        squares = jnp.sum(memory_out * memory_out, axis=1, keepdims=True)
        sqcol[rows, :] = jnp.broadcast_to(squares, (192, 128))
        mob[rows, :] = memory_out.astype(bf16)

    with scope("rs_start_head"):
        rs_start(*head_set, prepare=heads)
    ss[me] = sqcol[...].T[0:1]
    for k in range(1, NTP):
        send(ss.at[me], ss.at[me], ss_s.at[k], ss_r.at[k], lax.rem(me + k, NTP))
    with scope("rs_mid_head"):
        rs_mid(*head_set)
    for k in range(1, NTP):
        got(ss.at[lax.rem(me + NTP - k, NTP)], ss_r.at[k], "w_ss")
    total = ss[0]
    for k in range(1, NTP):
        total = total + ss[k]
    factor = lax.rsqrt(total / (NTP * VAL) + EPS)
    scol[...] = jnp.broadcast_to(factor, (128, BLK)).T
    got(x_c.at[y], rc_r.at[3])
    for k in range(4):
        got(gr_c.at[k], rc_r.at[6 + k], "w_gc")
    got(x_h.at[y], rh_r.at[3])
    factor = scol[pl.ds(pl.multiple_of(me * ROWS, 8), ROWS), 0:1]
    for k in range(2):
        cs = slice(k * COLS, (k + 1) * COLS)
        conv_sum = here(pb_c, x_c, cs) + gr_c[k].astype(f32) + gr_c[2 + k].astype(f32)
        fin[:, cs] = conv_sum + factor * here(pb_h, x_h, cs)
    for k in (1, 2, 0, 3):
        got(gr_h.at[k], rh_r.at[6 + k], "w_gh")
    with scope("final"):
        for k in range(2):
            cs = slice(k * COLS, (k + 1) * COLS)
            rest_sum = gr_h[k].astype(f32) + gr_h[2 + k].astype(f32)
            out[:, cs] = (fin[:, cs] + factor * rest_sum).astype(bf16)

    for cp in sends:
        cp.wait_send()
    edge.wait_send()

    def sent(ref, sem):
        pltpu.make_async_remote_copy(
            src_ref=ref, dst_ref=ref, send_sem=sem, recv_sem=sem,
            device_id=(sp, sib), device_id_type=MESH,
        ).wait_send()

    sent(aux.at[rest], aux_s)
    sent(st.at[rest], st_s)
    sent(cv.at[rest], cr_s)


def solution(mesh):
    n_sp = mesh.shape["sp"]
    tpd = TILES // n_sp
    vmem = pl.BlockSpec(memory_space=pltpu.VMEM)
    hbm = pl.BlockSpec(memory_space=pl.ANY)
    dma = pltpu.SemaphoreType.DMA

    def rs_bufs():
        return [
            pltpu.VMEM((BLK, D), bf16),
            pltpu.VMEM((4, ROWS, D), bf16),
            pltpu.VMEM((2, ROWS, COLS), bf16),
            pltpu.VMEM((2, ROWS, COLS), bf16),
            pltpu.VMEM((4, ROWS, COLS), bf16),
            pltpu.VMEM((4, ROWS, COLS), bf16),
        ]

    scratch = [
        pltpu.VMEM((ROWS, D), bf16),
        pltpu.VMEM((1, D), f32),
        pltpu.VMEM((NTP, D), bf16),
        pltpu.VMEM((NTP, D), bf16),
        pltpu.VMEM((1, NTP), f32),
        pltpu.VMEM((1, BLK), f32),
        pltpu.VMEM((3, NTP * CH), f32),
        pltpu.VMEM((KEY, VAL), f32),
        pltpu.VMEM((1, KEY), f32),
        pltpu.VMEM((BLK, D), bf16),
        pltpu.VMEM((D, 1408), bf16),
        pltpu.VMEM((VAL, D), bf16),
        pltpu.VMEM((CH, D), bf16),
        pltpu.VMEM((BLK, 1280), bf16),
        pltpu.VMEM((BLK, 128), f32),
        pltpu.VMEM((8, BLK), f32),
        pltpu.VMEM((BLK, 128), f32),
        pltpu.VMEM((n_sp, tpd, 8, 128), f32),
        pltpu.VMEM((n_sp, tpd, 8, 128), f32),
        pltpu.VMEM((n_sp, 1, 384), f32),
        pltpu.VMEM((n_sp, tpd, 8, 128), f32),
        pltpu.VMEM((n_sp, tpd, 8, 128), f32),
        pltpu.VMEM((n_sp, 1, 128), f32),
        pltpu.VMEM((n_sp, 1, 128), f32),
        pltpu.VMEM((KEY, VAL), f32),
        pltpu.VMEM((BLK, VAL), f32),
        pltpu.VMEM((BLK, 128), f32),
        pltpu.VMEM((BLK, VAL), bf16),
        pltpu.VMEM((BLK, CH), bf16),
        pltpu.VMEM((BLK + 8, CH), f32),
        pltpu.VMEM((16, CH), bf16),
        pltpu.VMEM((16, CH), bf16),
        pltpu.VMEM((NTP, 1, BLK), f32),
        pltpu.VMEM((BLK, 128), f32),
        pltpu.VMEM((BLK, 128), f32),
        pltpu.VMEM((ROWS, D), f32),
        *rs_bufs(),
        *rs_bufs(),
        dma((8,)),
        dma((9,)),
        dma((13,)),
        dma((13,)),
        dma(()),
        dma(()),
        dma(()),
        dma(()),
        dma(()),
        dma(()),
        dma(()),
        dma(()),
        dma((NTP,)),
        dma((NTP,)),
        dma((10,)),
        dma((10,)),
        dma((10,)),
        dma((10,)),
    ]

    def per_device(
        tokens, in_gain, w_query, w_key, w_value, w_input_gate, w_forget_gate, forget_bias,
        forget_extra, w_conv_gate, w_conv_left, w_conv_right, conv_taps, first_memory,
        first_norm, w_out_memory, w_out_conv,
    ):
        return pl.pallas_call(
            functools.partial(kernel, n_sp),
            out_shape=jax.ShapeDtypeStruct((ROWS, D), bf16),
            in_specs=[hbm] * 17,
            out_specs=vmem,
            scratch_shapes=scratch,
            compiler_params=pltpu.CompilerParams(
                collective_id=0, has_side_effects=True, vmem_limit_bytes=60 * 1024 * 1024
            ),
        )(
            tokens, in_gain.reshape(1, D), w_input_gate.T, w_forget_gate.T,
            forget_bias.reshape(1, NTP),
            forget_extra.reshape(1, BLK), conv_taps, first_memory.reshape(KEY, VAL), first_norm,
            w_query, w_key, w_value, w_conv_gate, w_conv_left, w_conv_right,
            w_out_memory, w_out_conv,
        )

    placed = (
        P(("sp", "tp"), None),
        P(),
        P(None, "tp"),
        P(None, "tp"),
        P(None, "tp"),
        P(),
        P(),
        P(),
        P("sp", "tp"),
        P(None, "tp"),
        P(None, "tp"),
        P(None, "tp"),
        P(),
        P("tp", None, None),
        P("tp", None),
        P("tp", None),
        P("tp", None),
    )
    return jax.shard_map(
        per_device, mesh=mesh, in_specs=placed, out_specs=P(("sp", "tp"), None), check_vma=False
    )
```

time: 75.1 us -> 70.4 us (0.937)
  Pallas kernels: 73.2 us -> 68.5 us
    pallas_call x1, Pallas kernels: 73.2 us -> 68.5 us  [per_device(): pl.pallas_call(functools.partial(kernel, n_sp), out_shape=jax.ShapeDtypeS...]
where the time goes in v2:
time: 70.4 us; the launch traced here: 70.3 us
  Pallas kernels  68.5 us (97%)
  local copies, waits for them, and re-layouts  1.77 us (3%)
    pallas_call x1, Pallas kernels, per_device(): pl.pallas_call(functools.partial(kernel, n_sp), out_shape=jax.ShapeDtypeS...  68.5 us
    unnamed x1, local copies, waits for them, and re-layouts  1.77 us

profile of v2, /device:TPU:1, one launch (start us, length us, event | category | flops | bytes accessed | tf_op | source)
XLA Modules:
  0.0 70.3 jit_solution(12277396664968637145)
XLA Ops:
  0.0 68.5 %shard_map.163 = bf16[96,2048]{1,0:T(8,128)(2,1)} custom-call(bf16[96,2048]{1,0:T(8,128)(2,1)} %tok_h.1, f32[1,2048]{1,0:T(1,128)} %bitcast.9, bf16[8,2048]{1,0:T(8,128)(2,1)} %bitcast.7, bf16[8,2048]{1,0:T(8,128)(2,1)} %bitcast.8, f32[1,8]{1,0:T(1,128)} %bitcast.11, f32[1,768]{1,0:T(1,128)} %bitcast.10, f32[3,2048]{1,0:T(4,128)} %taps_h.1, ...), custom_call_target="tpu_custom_call" | custom-call | tf_op jit(solution)/shard_map/pallas_call | solution.py:586
  68.5 1.8 %copy.19 = bf16[96,2048]{1,0:T(8,128)(2,1)} copy(bf16[96,2048]{1,0:T(8,128)(2,1)} %shard_map.163) | data formatting | bytes 786432

commit v3 on v2

--- a/solution.py
+++ b/solution.py
@@ -28,6 +28,14 @@
     return lax.dot_general(a, b, (((1,), (1,)), ((), ())), preferred_element_type=f32)
 
 
+def groups_of(n_sp):
+    if n_sp == 32:
+        return ((0, 8), (8, 16), (16, 32))
+    if n_sp == 4:
+        return ((0, 2), (2, 4))
+    return ((0, n_sp),)
+
+
 def dot(a, b):
     return jnp.dot(a, b, preferred_element_type=f32)
 
@@ -39,14 +47,15 @@
     out,
     tok, gain, wi, wf, bias, fextra, taps, fmem, fnorm,
     x, w_all, wom_v, woc_v,
-    proj, gates, urow, cmcol, st, rv, aux, cv, cr, mh, nh, cmem, pv, rs,
+    proj, gates, urow, cmcol, st, rv, aux, cv, cr, mh, nh, m_at, n_at,
+    ex, ea, px, pa, cmem, pv, rs,
     mob, cbr, prod, eb, er, ss, scol, sqcol, fin,
     pb_c, x_c, fs_c, fr_c, gs_c, gr_c,
     pb_h, x_h, fs_h, fr_h, gs_h, gr_h,
     wsem, isem, ag_s, ag_r, aux_s, aux_r, st_s, st_r, cr_s, cr_r, ed_s, ed_r, ss_s, ss_r,
-    rc_s, rc_r, rh_s, rh_r,
+    rc_s, rc_r, rh_s, rh_r, ex_s, px_r, ea_s, pa_r, ready, ready_edge,
 ):
-    tpd = TILES // n_sp
+    groups = groups_of(n_sp)
     scope = jax.named_scope
     sp = lax.axis_index("sp")
     me = lax.axis_index("tp")
@@ -56,8 +65,28 @@
     yn_y, yp_y, yo_y = lax.rem(y + 1, 4), lax.rem(y + 3, 4), lax.rem(y + 2, 4)
     yn, yp = yn_y * 2 + c, yp_y * 2 + c
 
-    def sp_peer(k):
-        return lax.rem(sp + k, n_sp)
+    def in_group(g):
+        return jnp.logical_and(sp >= groups[g][0], sp < groups[g][1])
+
+    def mates(g, start):
+        lo, hi = groups[g]
+        n = hi - lo
+        for k in range(1, n):
+            far = n // 2 + (k // 2 if k % 2 else -(k // 2))
+            start(lo + lax.rem(sp - lo + far, n))
+
+    def following(g):
+        lo, hi = groups[g]
+        if g + 1 == len(groups):
+            return []
+        at, end = groups[g + 1]
+        ratio = (end - at) // (hi - lo)
+        return [at + (sp - lo) * ratio + q for q in range(ratio)]
+
+    def preceding(g):
+        lo, hi = groups[g]
+        at, end = groups[g - 1]
+        return at + (sp - lo) // ((hi - lo) // (end - at))
 
     inputs = [
         pltpu.make_async_copy(src, dst, isem.at[i])
@@ -91,11 +120,23 @@
             barrier, inc=1, device_id=(sp, lax.rem(me + k, NTP)), device_id_type=MESH
         )
 
-    def greet(k, _):
-        pl.semaphore_signal(barrier, inc=1, device_id=(sp_peer(k), me), device_id_type=MESH)
-        return 0
-
-    lax.fori_loop(1, n_sp, greet, 0)
+    def greet(p):
+        pl.semaphore_signal(barrier, inc=1, device_id=(p, me), device_id_type=MESH)
+
+    for g, (lo, hi) in enumerate(groups):
+
+        @pl.when(in_group(g))
+        def _(g=g):
+            mates(g, greet)
+            for p in following(g):
+                greet(p)
+
+        if hi < n_sp:
+
+            @pl.when(sp == hi - 1)
+            def _():
+                greet(sp + 1)
+
     for cp in inputs[4:]:
         cp.start()
     for w in weights:
@@ -110,8 +151,21 @@
         t = tok[...].astype(f32)
         scale = lax.rsqrt(jnp.mean(t * t, axis=1, keepdims=True) + EPS)
         x[pl.ds(pl.multiple_of(c * ROWS, 16), ROWS), :] = (t * scale * gain[...]).astype(bf16)
+    prod[0:8, :] = jnp.zeros((8, CH), f32)
+
     with scope("w_barrier"):
-        pl.semaphore_wait(barrier, NTP - 1 + n_sp - 1)
+        for g, (lo, hi) in enumerate(groups):
+            count = NTP - 1 + hi - lo - 1 + (1 if lo else 0)
+
+            @pl.when(jnp.logical_and(in_group(g), jnp.logical_or(sp != lo, lo == 0)))
+            def _(count=count):
+                pl.semaphore_wait(barrier, count)
+
+            if lo:
+
+                @pl.when(sp == lo)
+                def _(count=count):
+                    pl.semaphore_wait(barrier, count + 1)
 
     sends = []
 
@@ -139,6 +193,19 @@
     ag(2 * c + 1, 8 + c, 1, yn)
     ag(2 * c, 10 + c, 4, yp)
     ag(2 * c, 2 * c, 6, sib, 2)
+    def tell(sem, p):
+        pl.semaphore_signal(sem, inc=1, device_id=(p, me), device_id_type=MESH)
+
+    for g, (lo, hi) in enumerate(groups):
+        if lo:
+
+            @pl.when(in_group(g))
+            def _(g=g):
+                tell(ready, preceding(g))
+
+            @pl.when(sp == lo)
+            def _():
+                tell(ready_edge, sp - 1)
 
     inputs[2].wait()
     inputs[3].wait()
@@ -157,17 +224,40 @@
             for k, base in enumerate(bases):
                 rows = pl.ds(pl.multiple_of(base, 16), HALF)
                 piece = res[k * HALF : (k + 1) * HALF]
-                if hi <= 1280:
+                if lo == 512:
+                    left = piece[:, :CH].astype(bf16).astype(f32)
+                    right = piece[:, CH:].astype(bf16).astype(f32)
+                    at = pl.ds(pl.multiple_of(base + 8, 8), HALF)
+                    prod[at, :] = (left * right).astype(bf16).astype(f32)
+                elif hi <= 1280:
                     proj[rows, lo:hi] = piece.astype(bf16)
                 else:
                     gates[rows, :] = piece[:, 1280 - lo :]
                     if lo < 1280:
                         proj[rows, lo:1280] = piece[:, : 1280 - lo].astype(bf16)
 
+    edge = pltpu.make_async_remote_copy(
+        src_ref=eb, dst_ref=er, send_sem=ed_s, recv_sem=ed_r,
+        device_id=(lax.rem(sp + 1, n_sp), me), device_id_type=MESH,
+    )
+
+    def send_edge(where):
+        @pl.when(jnp.logical_and(y == where, sp < n_sp - 1))
+        def _():
+            eb[...] = prod[BLK - 8 :, :].astype(bf16)
+            for lo, hi in groups[:-1]:
+
+                @pl.when(sp == hi - 1)
+                def _():
+                    pl.semaphore_wait(ready_edge, 1)
+
+            edge.start()
+
     every = ((0, 512), (512, 1024), (1024, 1408))
     got(slots(2 * other, 2), ag_r.at[6], "w_ag6")
     with scope("proj_0"):
         project(0, [y * 192 + HALF * k for k in range(4)], every)
+        send_edge(3)
     got(slots(4 + c), ag_r.at[0], "w_ag0")
     ag(4 + c, 12 + c, 2, yn)
     ag(4 + c, 4 + c, 7, sib)
@@ -182,6 +272,7 @@
             [yp_y * 192, yp_y * 192 + ROWS, yn_y * 192 + HALF, yn_y * 192 + ROWS + HALF],
             every,
         )
+        send_edge(2)
     got(slots(8 + c), ag_r.at[1], "w_ag1")
     ag(8 + c, 8 + c, 9, sib)
     got(slots(10 + c), ag_r.at[4], "w_ag4")
@@ -194,6 +285,7 @@
             [yp_y * 192 + HALF, yp_y * 192 + ROWS + HALF, yn_y * 192, yn_y * 192 + ROWS],
             every,
         )
+        send_edge(0)
     got(slots(12 + c), ag_r.at[2], "w_ag2")
     ag(12 + c, 12 + c, 11, sib)
     got(slots(14 + c), ag_r.at[5], "w_ag5")
@@ -258,24 +350,14 @@
         aux[sp] = jnp.concatenate([d_lanes, m_lanes, block_norm], axis=1)
         for p in range(TILES):
             i, j = p // 2, p % 2
-            st[p // tpd, p % tpd] = mem[8 * i : 8 * i + 8, 128 * j : 128 * j + 128]
-
-    def over_peers(start):
-        half = n_sp // 2
-        start(half)
-
-        def both(i, _):
-            start(half + i)
-            start(half - i)
-            return 0
-
-        lax.fori_loop(1, half, both, 0)
-
-    def start_state(k):
-        p = sp_peer(k)
+            st[p] = mem[8 * i : 8 * i + 8, 128 * j : 128 * j + 128]
+
+    def start_state(g, p):
+        lo, hi = groups[g]
+        n = TILES // (hi - lo)
         pltpu.make_async_remote_copy(
-            src_ref=st.at[p], dst_ref=rv.at[sp], send_sem=st_s, recv_sem=st_r,
-            device_id=(p, me), device_id_type=MESH,
+            src_ref=st.at[pl.ds((p - lo) * n, n)], dst_ref=rv.at[sp - lo, pl.ds(0, n)],
+            send_sem=st_s, recv_sem=st_r, device_id=(p, me), device_id_type=MESH,
         ).start()
         pltpu.make_async_remote_copy(
             src_ref=aux.at[sp], dst_ref=aux.at[sp], send_sem=aux_s, recv_sem=aux_r,
@@ -283,21 +365,174 @@
         ).start()
 
     with scope("send_state"):
-        over_peers(start_state)
-    rv[sp] = st[sp]
-
-    with scope("proj_lr"):
+        for g, (lo, hi) in enumerate(groups):
+
+            @pl.when(in_group(g))
+            def _(g=g, lo=lo, hi=hi):
+                mates(g, functools.partial(start_state, g))
+                n = TILES // (hi - lo)
+                for k in range(n):
+                    rv[sp - lo, k] = st[(sp - lo) * n + k]
+
+    with scope("proj_lrg"):
         project(3, last, ((512, 1024),))
-        product = (proj[:, 512:768].astype(f32) * proj[:, 768:1024].astype(f32)).astype(bf16)
-        eb[...] = product[BLK - 16 :]
-        prod[8:, :] = product.astype(f32)
-    edge = pltpu.make_async_remote_copy(
-        src_ref=eb, dst_ref=er, send_sem=ed_s, recv_sem=ed_r,
-        device_id=(sp_peer(1), me), device_id_type=MESH,
-    )
-    edge.start()
-    with scope("proj_g"):
+        send_edge(1)
         project(3, last, ((1024, 1280),))
+
+    def own(d):
+        return pl.ds(pl.multiple_of((d * 2 + c) * ROWS, 16), ROWS)
+
+    def his(d):
+        return pl.ds(pl.multiple_of((d * 2 + 1 - c) * ROWS, 16), ROWS)
+
+    def rs_rows(n, d, a, wv_, pb, xb, s_, r_, prepare):
+        rows = pl.ds(pl.multiple_of(d * 192, 64), 192)
+        prepare(n, d)
+        for lo in range(0, D, COLS):
+            pb[rows, lo : lo + COLS] = dot(a[rows, :], wv_[:, lo : lo + COLS]).astype(bf16)
+        send(pb.at[his(d)], xb.at[d], s_.at[n], r_.at[n], sib)
+
+    def rs_first(a, wv_, pb, xb, fs, fr, gs, gr, s_, r_, prepare):
+        rs_rows(0, yo_y, a, wv_, pb, xb, s_, r_, prepare)
+        rs_rows(1, yn_y, a, wv_, pb, xb, s_, r_, prepare)
+        got(xb.at[yo_y], r_.at[0], "w_x0")
+        tot = pb[own(yo_y), :].astype(f32) + xb[yo_y].astype(f32)
+        fs[0] = tot[:, :COLS].astype(bf16)
+        fs[1] = tot[:, COLS:].astype(bf16)
+        send(fs.at[0], fr.at[0], s_.at[4], r_.at[4], yn)
+        send(fs.at[1], fr.at[1], s_.at[5], r_.at[5], yp)
+
+    def rs_second(a, wv_, pb, xb, fs, fr, gs, gr, s_, r_, prepare):
+        rs_rows(2, yp_y, a, wv_, pb, xb, s_, r_, prepare)
+        rs_rows(3, y, a, wv_, pb, xb, s_, r_, prepare)
+        got(xb.at[yn_y], r_.at[1], "w_x1")
+        tot = pb[own(yn_y), COLS:].astype(f32) + xb[yn_y, :, COLS:].astype(f32)
+        gs[1] = tot.astype(bf16)
+        send(gs.at[1], gr.at[1], s_.at[7], r_.at[7], yn)
+        got(xb.at[yp_y], r_.at[2], "w_x2")
+        tot = pb[own(yp_y), :COLS].astype(f32) + xb[yp_y, :, :COLS].astype(f32)
+        gs[2] = tot.astype(bf16)
+        send(gs.at[2], gr.at[2], s_.at[8], r_.at[8], yp)
+
+    def rs_mid(a, wv_, pb, xb, fs, fr, gs, gr, s_, r_):
+        got(fr.at[0], r_.at[4], "w_f0")
+        tot = pb[own(yn_y), :COLS].astype(f32) + xb[yn_y, :, :COLS].astype(f32)
+        gs[0] = (tot + fr[0].astype(f32)).astype(bf16)
+        send(gs.at[0], gr.at[0], s_.at[6], r_.at[6], yn)
+        got(fr.at[1], r_.at[5], "w_f1")
+        tot = pb[own(yp_y), COLS:].astype(f32) + xb[yp_y, :, COLS:].astype(f32)
+        gs[3] = (tot + fr[1].astype(f32)).astype(bf16)
+        send(gs.at[3], gr.at[3], s_.at[9], r_.at[9], yp)
+
+    def here(pb, xb, cs):
+        return pb[own(y), cs].astype(f32) + xb[y, :, cs].astype(f32)
+
+    def filtered(n, d):
+        @pl.when(jnp.logical_and(d == 0, sp > 0))
+        def _():
+            with scope("w_edge"):
+                edge.wait_recv()
+            prod[0:8, :] = er[8:16, :].astype(f32)
+
+        rows = pl.ds(pl.multiple_of(d * 192, 64), 192)
+        mine = pl.ds(pl.multiple_of(me * CH, CH), CH)
+        near = prod[pl.ds(pl.multiple_of(d * 192, 64), 200), :]
+        f = taps[0:1, mine] * near[6:198]
+        f = f + taps[1:2, mine] * near[7:199]
+        f = f + taps[2:3, mine] * near[8:200]
+        cbr[rows, :] = (proj[rows, 1024:1280].astype(f32) * f).astype(bf16)
+
+    conv_set = (cbr, woc_v, pb_c, x_c, fs_c, fr_c, gs_c, gr_c, rc_s, rc_r)
+    head_set = (mob, wom_v, pb_h, x_h, fs_h, fr_h, gs_h, gr_h, rh_s, rh_r)
+    weights[6].wait()
+    weights[7].wait()
+    def start_carry(g, p):
+        lo, hi = groups[g]
+        n = TILES // (hi - lo)
+        pltpu.make_async_remote_copy(
+            src_ref=cv.at[p - lo, pl.ds(0, n)], dst_ref=cr.at[pl.ds((sp - lo) * n, n)],
+            send_sem=cr_s, recv_sem=cr_r, device_id=(p, me), device_id_type=MESH,
+        ).start()
+
+    def pass_on(g):
+        lo, hi = groups[g]
+        out_ = []
+        for q, p in enumerate(following(g)):
+            n = TILES // (groups[g + 1][1] - groups[g + 1][0])
+            out_ += [
+                pltpu.make_async_remote_copy(
+                    src_ref=ex.at[pl.ds(q * n, n)], dst_ref=px.at[pl.ds(0, n)],
+                    send_sem=ex_s.at[q], recv_sem=px_r, device_id=(p, me), device_id_type=MESH,
+                ),
+                pltpu.make_async_remote_copy(
+                    src_ref=ea, dst_ref=pa, send_sem=ea_s.at[q], recv_sem=pa_r,
+                    device_id=(p, me), device_id_type=MESH,
+                ),
+            ]
+        return out_
+
+    def recurrence(g):
+        lo, hi = groups[g]
+        n = TILES // (hi - lo)
+        with scope("w_state"):
+            if hi - lo > 1:
+                got(aux.at[pl.ds(0, hi - lo - 1)], aux_r)
+                got(rv.at[pl.ds(0, hi - lo - 1), pl.ds(0, n)], st_r)
+        if lo:
+            with scope("w_prefix"):
+                got(px.at[pl.ds(0, n)], px_r)
+                got(pa, pa_r)
+            tiles = [px[k] for k in range(n)]
+            run_m = pa[:, 0:128]
+            run_n = pa[:, 128:256]
+        else:
+            tiles = []
+            for k in range(n):
+                p = (sp - lo) * n + k
+                r_i = pl.ds(pl.multiple_of((p // 2) * 8, 8), 8)
+                c_i = pl.ds(pl.multiple_of(lax.rem(p, 2) * 128, 128), 128)
+                tiles.append(fmem[r_i, c_i])
+            run_m = jnp.zeros((1, 128), f32)
+            run_n = fnorm[...]
+        last_one = hi == n_sp
+        for b in range(lo, hi):
+            for k in range(n):
+                cv[b - lo, k] = tiles[k]
+            mh[b - lo] = run_m
+            nh[b - lo] = run_n
+            if b < hi - 1 or not last_one:
+                row = aux[b]
+                new_m = jnp.maximum(run_m + row[:, 0:128], row[:, 128:256])
+                old = jnp.exp(run_m + row[:, 0:128] - new_m)
+                new = jnp.exp(row[:, 128:256] - new_m)
+                tiles = [old * tiles[k] + new * rv[b - lo, k] for k in range(n)]
+                run_n = old * run_n + new * row[:, 256:384]
+                run_m = new_m
+        if not last_one:
+            for k in range(n):
+                ex[k] = tiles[k]
+            ea[...] = jnp.concatenate([run_m, run_n], axis=1)
+            with scope("w_ready"):
+                pl.semaphore_wait(ready, len(following(g)))
+            for cp in pass_on(g):
+                cp.start()
+        with scope("send_carry"):
+            mates(g, functools.partial(start_carry, g))
+        for k in range(n):
+            cr[(sp - lo) * n + k] = cv[sp - lo, k]
+        m_at[...] = mh[sp - lo]
+        n_at[...] = nh[sp - lo]
+
+    def take(g):
+        @pl.when(in_group(g))
+        def _():
+            recurrence(g)
+
+    with scope("rs_first_conv"):
+        rs_first(*conv_set, filtered)
+    take(0)
+    with scope("rs_second_conv"):
+        rs_second(*conv_set, filtered)
 
     with scope("mixing"):
         top = jnp.broadcast_to(u_row, (8, BLK))
@@ -325,114 +560,26 @@
             pv[r0 : r0 + 256, :] = acc
             rs[r0 : r0 + 256, :] = jnp.broadcast_to(tot, (256, 128))
 
-    with scope("w_edge"):
-        edge.wait_recv()
-    with scope("filter"):
-        prod[0:8, :] = jnp.where(sp > 0, er[...].astype(f32)[8:16], 0.0)
-        mine = pl.ds(pl.multiple_of(me * CH, CH), CH)
-        filtered = taps[0:1, mine] * prod[6 : 6 + BLK, :]
-        filtered = filtered + taps[1:2, mine] * prod[7 : 7 + BLK, :]
-        filtered = filtered + taps[2:3, mine] * prod[8 : 8 + BLK, :]
-        cbr[...] = (proj[:, 1024:1280].astype(f32) * filtered).astype(bf16)
-
-    def own(d):
-        return pl.ds(pl.multiple_of((d * 2 + c) * ROWS, 16), ROWS)
-
-    def his(d):
-        return pl.ds(pl.multiple_of((d * 2 + 1 - c) * ROWS, 16), ROWS)
-
-    def rs_start(a, wv_, pb, xb, fs, fr, gs, gr, s_, r_, prepare=None):
-        for n, d in ((0, yo_y), (1, yn_y), (2, yp_y), (3, y)):
-            rows = pl.ds(pl.multiple_of(d * 192, 64), 192)
-            if prepare is not None:
-                prepare(rows)
-            for lo in range(0, D, COLS):
-                pb[rows, lo : lo + COLS] = dot(a[rows, :], wv_[:, lo : lo + COLS]).astype(bf16)
-            send(pb.at[his(d)], xb.at[d], s_.at[n], r_.at[n], sib)
-            if n == 1:
-                got(xb.at[yo_y], r_.at[0], "w_x0")
-                tot = pb[own(yo_y), :].astype(f32) + xb[yo_y].astype(f32)
-                fs[0] = tot[:, :COLS].astype(bf16)
-                fs[1] = tot[:, COLS:].astype(bf16)
-                send(fs.at[0], fr.at[0], s_.at[4], r_.at[4], yn)
-                send(fs.at[1], fr.at[1], s_.at[5], r_.at[5], yp)
-        got(xb.at[yn_y], r_.at[1], "w_x1")
-        tot = pb[own(yn_y), COLS:].astype(f32) + xb[yn_y, :, COLS:].astype(f32)
-        gs[1] = tot.astype(bf16)
-        send(gs.at[1], gr.at[1], s_.at[7], r_.at[7], yn)
-        got(xb.at[yp_y], r_.at[2], "w_x2")
-        tot = pb[own(yp_y), :COLS].astype(f32) + xb[yp_y, :, :COLS].astype(f32)
-        gs[2] = tot.astype(bf16)
-        send(gs.at[2], gr.at[2], s_.at[8], r_.at[8], yp)
-
-    def rs_mid(a, wv_, pb, xb, fs, fr, gs, gr, s_, r_):
-        got(fr.at[0], r_.at[4], "w_f0")
-        tot = pb[own(yn_y), :COLS].astype(f32) + xb[yn_y, :, :COLS].astype(f32)
-        gs[0] = (tot + fr[0].astype(f32)).astype(bf16)
-        send(gs.at[0], gr.at[0], s_.at[6], r_.at[6], yn)
-        got(fr.at[1], r_.at[5], "w_f1")
-        tot = pb[own(yp_y), COLS:].astype(f32) + xb[yp_y, :, COLS:].astype(f32)
-        gs[3] = (tot + fr[1].astype(f32)).astype(bf16)
-        send(gs.at[3], gr.at[3], s_.at[9], r_.at[9], yp)
-
-    def here(pb, xb, cs):
-        return pb[own(y), cs].astype(f32) + xb[y, :, cs].astype(f32)
-
-    conv_set = (cbr, woc_v, pb_c, x_c, fs_c, fr_c, gs_c, gr_c, rc_s, rc_r)
-    head_set = (mob, wom_v, pb_h, x_h, fs_h, fr_h, gs_h, gr_h, rh_s, rh_r)
-    weights[6].wait()
-    weights[7].wait()
-    with scope("rs_start_conv"):
-        rs_start(*conv_set)
-
-    rest = pl.ds(0, n_sp - 1)
-    got(aux.at[rest], aux_r, "w_aux")
-    got(rv.at[rest], st_r, "w_state")
-    first = []
-    for k in range(tpd):
-        p = sp * tpd + k
-        r_i = pl.ds(pl.multiple_of((p // 2) * 8, 8), 8)
-        c_i = pl.ds(pl.multiple_of(lax.rem(p, 2) * 128, 128), 128)
-        first.append(fmem[r_i, c_i])
-    run_m = jnp.zeros((1, 128), f32)
-    run_n = fnorm[...]
-    for b in range(n_sp):
-        for k in range(tpd):
-            cv[b, k] = first[k]
-        mh[b] = run_m
-        nh[b] = run_n
-        if b < n_sp - 1:
-            row = aux[b]
-            new_m = jnp.maximum(run_m + row[:, 0:128], row[:, 128:256])
-            old = jnp.exp(run_m + row[:, 0:128] - new_m)
-            new = jnp.exp(row[:, 128:256] - new_m)
-            first = [old * first[k] + new * rv[b, k] for k in range(tpd)]
-            run_n = old * run_n + new * row[:, 256:384]
-            run_m = new_m
-
-    def start_carry(k):
-        p = sp_peer(k)
-        pltpu.make_async_remote_copy(
-            src_ref=cv.at[p], dst_ref=cr.at[sp], send_sem=cr_s, recv_sem=cr_r,
-            device_id=(p, me), device_id_type=MESH,
-        ).start()
-
-    with scope("send_carry"):
-        over_peers(start_carry)
-    cr[sp] = cv[sp]
+    for g in range(1, len(groups)):
+        take(g)
     with scope("rs_mid_conv"):
         rs_mid(*conv_set)
 
-    got(cr.at[rest], cr_r, "w_carry")
+    for g, (lo, hi) in enumerate(groups):
+
+        @pl.when(in_group(g))
+        def _(lo=lo, hi=hi):
+            got(cr.at[pl.ds(0, TILES - TILES // (hi - lo))], cr_r, "w_carry")
+
     with scope("carry"):
         for p in range(TILES):
             i, j = p // 2, p % 2
-            cmem[8 * i : 8 * i + 8, 128 * j : 128 * j + 128] = cr[p // tpd, p % tpd]
+            cmem[8 * i : 8 * i + 8, 128 * j : 128 * j + 128] = cr[p]
         carry = cmem[...]
         high = carry.astype(bf16)
         low = (carry - high.astype(f32)).astype(bf16)
-        m_in = mh[sp][:, 0:1]
-        n_in = nh[sp]
+        m_in = m_at[:, 0:1]
+        n_in = n_at[...]
         n_1 = n_in.astype(bf16).astype(f32)
         n_2 = (n_in - n_1).astype(bf16).astype(f32)
         n_3 = n_in - n_1 - n_2
@@ -441,7 +588,8 @@
             sub16 == 0, n_1, jnp.where(sub16 == 1, n_2, jnp.where(sub16 == 2, n_3, 0.0))
         ).astype(bf16)
 
-    def heads(rows):
+    def heads(n, d):
+        rows = pl.ds(pl.multiple_of(d * 192, 64), 192)
         q = proj[rows, 128:256]
         cm = cmcol[rows, 0:1]
         peak = jnp.maximum(cm, m_in)
@@ -456,8 +604,10 @@
         sqcol[rows, :] = jnp.broadcast_to(squares, (192, 128))
         mob[rows, :] = memory_out.astype(bf16)
 
-    with scope("rs_start_head"):
-        rs_start(*head_set, prepare=heads)
+    with scope("rs_first_head"):
+        rs_first(*head_set, heads)
+    with scope("rs_second_head"):
+        rs_second(*head_set, heads)
     ss[me] = sqcol[...].T[0:1]
     for k in range(1, NTP):
         send(ss.at[me], ss.at[me], ss_s.at[k], ss_r.at[k], lax.rem(me + k, NTP))
@@ -489,22 +639,34 @@
 
     for cp in sends:
         cp.wait_send()
-    edge.wait_send()
-
     def sent(ref, sem):
         pltpu.make_async_remote_copy(
             src_ref=ref, dst_ref=ref, send_sem=sem, recv_sem=sem,
             device_id=(sp, sib), device_id_type=MESH,
         ).wait_send()
 
-    sent(aux.at[rest], aux_s)
-    sent(st.at[rest], st_s)
-    sent(cv.at[rest], cr_s)
+    @pl.when(sp < n_sp - 1)
+    def _():
+        edge.wait_send()
+
+    for g, (lo, hi) in enumerate(groups):
+
+        @pl.when(in_group(g))
+        def _(g=g, lo=lo, hi=hi):
+            if hi - lo > 1:
+                rest = pl.ds(0, TILES - TILES // (hi - lo))
+                sent(st.at[rest], st_s)
+                sent(aux.at[pl.ds(0, hi - lo - 1)], aux_s)
+                sent(cr.at[rest], cr_s)
+            for cp in pass_on(g):
+                cp.wait_send()
 
 
 def solution(mesh):
     n_sp = mesh.shape["sp"]
-    tpd = TILES // n_sp
+    groups = groups_of(n_sp)
+    gmax = max(hi - lo for lo, hi in groups)
+    tmax = max(TILES // (hi - lo) for lo, hi in groups)
     vmem = pl.BlockSpec(memory_space=pltpu.VMEM)
     hbm = pl.BlockSpec(memory_space=pl.ANY)
     dma = pltpu.SemaphoreType.DMA
@@ -537,13 +699,19 @@
         pltpu.VMEM((BLK, 128), f32),
         pltpu.VMEM((8, BLK), f32),
         pltpu.VMEM((BLK, 128), f32),
-        pltpu.VMEM((n_sp, tpd, 8, 128), f32),
-        pltpu.VMEM((n_sp, tpd, 8, 128), f32),
+        pltpu.VMEM((TILES, 8, 128), f32),
+        pltpu.VMEM((gmax, tmax, 8, 128), f32),
         pltpu.VMEM((n_sp, 1, 384), f32),
-        pltpu.VMEM((n_sp, tpd, 8, 128), f32),
-        pltpu.VMEM((n_sp, tpd, 8, 128), f32),
-        pltpu.VMEM((n_sp, 1, 128), f32),
-        pltpu.VMEM((n_sp, 1, 128), f32),
+        pltpu.VMEM((gmax, tmax, 8, 128), f32),
+        pltpu.VMEM((TILES, 8, 128), f32),
+        pltpu.VMEM((gmax, 1, 128), f32),
+        pltpu.VMEM((gmax, 1, 128), f32),
+        pltpu.VMEM((1, 128), f32),
+        pltpu.VMEM((1, 128), f32),
+        pltpu.VMEM((tmax, 8, 128), f32),
+        pltpu.VMEM((1, 256), f32),
+        pltpu.VMEM((tmax, 8, 128), f32),
+        pltpu.VMEM((1, 256), f32),
         pltpu.VMEM((KEY, VAL), f32),
         pltpu.VMEM((BLK, VAL), f32),
         pltpu.VMEM((BLK, 128), f32),
@@ -576,6 +744,12 @@
         dma((10,)),
         dma((10,)),
         dma((10,)),
+        dma((4,)),
+        dma(()),
+        dma((4,)),
+        dma(()),
+        pltpu.SemaphoreType.REGULAR,
+        pltpu.SemaphoreType.REGULAR,
     ]
 
     def per_device(

time: 70.4 us -> 60.3 us (0.86)
  the two profiles are of different devices: /device:TPU:1 before, /device:TPU:129 now
where the time goes in v3:
time: 60.3 us; the launch traced here: 60.2 us
  Pallas kernels  58.4 us (97%)
  local copies, waits for them, and re-layouts  1.77 us (3%)
    pallas_call x1, Pallas kernels, per_device(): pl.pallas_call(functools.partial(kernel, n_sp), out_shape=jax.ShapeDtypeS...  58.4 us
    unnamed x1, local copies, waits for them, and re-layouts  1.77 us

profile of v3, /device:TPU:129, one launch (start us, length us, event | category | flops | bytes accessed | tf_op | source)
XLA Modules:
  0.0 60.2 jit_solution(746667577109542679)
XLA Ops:
  0.0 58.4 %shard_map.163 = bf16[96,2048]{1,0:T(8,128)(2,1)} custom-call(bf16[96,2048]{1,0:T(8,128)(2,1)} %tok_h.1, f32[1,2048]{1,0:T(1,128)} %bitcast.9, bf16[8,2048]{1,0:T(8,128)(2,1)} %bitcast.7, bf16[8,2048]{1,0:T(8,128)(2,1)} %bitcast.8, f32[1,8]{1,0:T(1,128)} %bitcast.11, f32[1,768]{1,0:T(1,128)} %bitcast.10, f32[3,2048]{1,0:T(4,128)} %taps_h.1, ...), custom_call_target="tpu_custom_call" | custom-call | tf_op jit(solution)/shard_map/pallas_call | solution.py:760
  58.4 1.8 %copy.19 = bf16[96,2048]{1,0:T(8,128)(2,1)} copy(bf16[96,2048]{1,0:T(8,128)(2,1)} %shard_map.163) | data formatting | bytes 786432

commit v4 on v3

--- a/solution.py
+++ b/solution.py
@@ -15,7 +15,7 @@
 HALF = 48
 BLK = 768
 NTP = 8
-TILES = 32
+TILES = 16
 COLS = 1024
 EPS = 1e-06
 SCALE = KEY ** (-0.5)
@@ -49,11 +49,11 @@
     x, w_all, wom_v, woc_v,
     proj, gates, urow, cmcol, st, rv, aux, cv, cr, mh, nh, m_at, n_at,
     ex, ea, px, pa, cmem, pv, rs,
-    mob, cbr, prod, eb, er, ss, scol, sqcol, fin,
-    pb_c, x_c, fs_c, fr_c, gs_c, gr_c,
-    pb_h, x_h, fs_h, fr_h, gs_h, gr_h,
+    mob, cbr, prod, eb, er, ss, scol, sqcol, own_c, own_h, part,
+    x_c, fs_c, fr_c, gs_c, gr_c,
+    x_h, fs_h, fr_h, gs_h, gr_h,
     wsem, isem, ag_s, ag_r, aux_s, aux_r, st_s, st_r, cr_s, cr_r, ed_s, ed_r, ss_s, ss_r,
-    rc_s, rc_r, rh_s, rh_r, ex_s, px_r, ea_s, pa_r, ready, ready_edge,
+    rc_s, rc_r, rh_s, rh_r, ex_s, px_r, ea_s, pa_r, ready, ready_edge, ow_s, ow_r,
 ):
     groups = groups_of(n_sp)
     scope = jax.named_scope
@@ -107,8 +107,8 @@
                 (wcl, w_all.at[:, pl.ds(512, 256)]),
                 (wcr, w_all.at[:, pl.ds(768, 256)]),
                 (wcg, w_all.at[:, pl.ds(1024, 256)]),
-                (woc, woc_v),
-                (wom, wom_v),
+                (woc, woc_v.at[pl.ds(0, CH), :]),
+                (wom, wom_v.at[pl.ds(0, VAL), :]),
             ]
         )
     ]
@@ -193,6 +193,8 @@
     ag(2 * c + 1, 8 + c, 1, yn)
     ag(2 * c, 10 + c, 4, yp)
     ag(2 * c, 2 * c, 6, sib, 2)
+    send(woc, woc_v.at[pl.ds(CH, CH), :], ow_s.at[0], ow_r.at[0], sib)
+    send(wom, wom_v.at[pl.ds(VAL, VAL), :], ow_s.at[1], ow_r.at[1], sib)
     def tell(sem, p):
         pl.semaphore_signal(sem, inc=1, device_id=(p, me), device_id_type=MESH)
 
@@ -207,8 +209,8 @@
             def _():
                 tell(ready_edge, sp - 1)
 
-    inputs[2].wait()
-    inputs[3].wait()
+    for cp in inputs[2:]:
+        cp.wait()
     gw = jnp.concatenate(
         [wi[...].astype(f32), wf[...].astype(f32), jnp.zeros((112, D), f32)], axis=0
     )
@@ -253,6 +255,74 @@
 
             edge.start()
 
+    def own(d):
+        return pl.ds(pl.multiple_of((d * 2 + c) * ROWS, 16), ROWS)
+
+    def his(d):
+        return pl.ds(pl.multiple_of((d * 2 + 1 - c) * ROWS, 16), ROWS)
+
+    order = (yo_y, yn_y, yp_y, y)
+
+    def rs_part(n, a, w, xb, s_, r_, prepare, kept=True):
+        prepare(n, order[n])
+        send(a.at[his(order[n])], xb.at[n], s_.at[n], r_.at[n], sib)
+        if not kept:
+            sends.pop()
+
+    def both(n, a, xb):
+        return jnp.concatenate([a[own(order[n]), :], xb[n]], axis=1)
+
+    def rs_first(a, w, xb, fs, fr, gs, gr, kept, s_, r_):
+        got(xb.at[0], r_.at[0], "w_x0")
+        lhs = both(0, a, xb)
+        for k, peer in ((0, yn), (1, yp)):
+            fs[k] = dot(lhs, w[:, k * COLS : (k + 1) * COLS]).astype(bf16)
+            send(fs.at[k], fr.at[k], s_.at[4 + k], r_.at[4 + k], peer)
+
+    def rs_second(a, w, xb, fs, fr, gs, gr, kept, s_, r_):
+        for n in (1, 2, 3):
+            got(xb.at[n], r_.at[n], "w_x123")
+        lhs = jnp.concatenate([both(n, a, xb) for n in (1, 2, 3)], axis=0)
+        res = dot(lhs, w[:, COLS:])
+        gs[1] = res[0:ROWS].astype(bf16)
+        send(gs.at[1], gr.at[1], s_.at[7], r_.at[7], yn)
+        part[1] = res[ROWS : 2 * ROWS]
+        kept[:, COLS:] = res[2 * ROWS :]
+        res = dot(lhs, w[:, :COLS])
+        gs[2] = res[ROWS : 2 * ROWS].astype(bf16)
+        send(gs.at[2], gr.at[2], s_.at[8], r_.at[8], yp)
+        part[0] = res[0:ROWS]
+        kept[:, :COLS] = res[2 * ROWS :]
+
+    def rs_mid(a, w, xb, fs, fr, gs, gr, kept, s_, r_):
+        got(fr.at[0], r_.at[4], "w_f0")
+        gs[0] = (part[0] + fr[0].astype(f32)).astype(bf16)
+        send(gs.at[0], gr.at[0], s_.at[6], r_.at[6], yn)
+        got(fr.at[1], r_.at[5], "w_f1")
+        gs[3] = (part[1] + fr[1].astype(f32)).astype(bf16)
+        send(gs.at[3], gr.at[3], s_.at[9], r_.at[9], yp)
+
+    def filtered(n, d):
+        @pl.when(jnp.logical_and(d == 0, sp > 0))
+        def _():
+            with scope("w_edge"):
+                edge.wait_recv()
+            prod[0:8, :] = er[8:16, :].astype(f32)
+
+        rows = pl.ds(pl.multiple_of(d * 192, 64), 192)
+        mine = pl.ds(pl.multiple_of(me * CH, CH), CH)
+        near = prod[pl.ds(pl.multiple_of(d * 192, 64), 200), :]
+        f = taps[0:1, mine] * near[6:198]
+        f = f + taps[1:2, mine] * near[7:199]
+        f = f + taps[2:3, mine] * near[8:200]
+        cbr[rows, :] = (proj[rows, 1024:1280].astype(f32) * f).astype(bf16)
+
+    conv_set = (cbr, woc_v, x_c, fs_c, fr_c, gs_c, gr_c, own_c, rc_s, rc_r)
+    head_set = (mob, wom_v, x_h, fs_h, fr_h, gs_h, gr_h, own_h, rh_s, rh_r)
+
+    def conv_part(n, kept=True):
+        rs_part(n, cbr, woc_v, x_c, rc_s, rc_r, filtered, kept)
+
     every = ((0, 512), (512, 1024), (1024, 1408))
     got(slots(2 * other, 2), ag_r.at[6], "w_ag6")
     with scope("proj_0"):
@@ -290,14 +360,14 @@
     ag(12 + c, 12 + c, 11, sib)
     got(slots(14 + c), ag_r.at[5], "w_ag5")
     ag(14 + c, 14 + c, 12, sib)
+    with scope("conv_early"):
+        conv_part(1)
     got(slots(12 + other), ag_r.at[11], "w_ag11")
     got(slots(14 + other), ag_r.at[12], "w_ag12")
     last = [yo_y * 192, yo_y * 192 + ROWS, yo_y * 192 + HALF, yo_y * 192 + ROWS + HALF]
     with scope("proj_3"):
         project(3, last, ((1280, 1408), (0, 512)))
 
-    for cp in inputs[4:]:
-        cp.wait()
     with scope("state"):
         g_t = gates[...].T
         sub = lax.broadcasted_iota(jnp.int32, (8, BLK), 0)
@@ -350,7 +420,7 @@
         aux[sp] = jnp.concatenate([d_lanes, m_lanes, block_norm], axis=1)
         for p in range(TILES):
             i, j = p // 2, p % 2
-            st[p] = mem[8 * i : 8 * i + 8, 128 * j : 128 * j + 128]
+            st[p] = mem[16 * i : 16 * i + 16, 128 * j : 128 * j + 128].astype(bf16)
 
     def start_state(g, p):
         lo, hi = groups[g]
@@ -379,73 +449,6 @@
         send_edge(1)
         project(3, last, ((1024, 1280),))
 
-    def own(d):
-        return pl.ds(pl.multiple_of((d * 2 + c) * ROWS, 16), ROWS)
-
-    def his(d):
-        return pl.ds(pl.multiple_of((d * 2 + 1 - c) * ROWS, 16), ROWS)
-
-    def rs_rows(n, d, a, wv_, pb, xb, s_, r_, prepare):
-        rows = pl.ds(pl.multiple_of(d * 192, 64), 192)
-        prepare(n, d)
-        for lo in range(0, D, COLS):
-            pb[rows, lo : lo + COLS] = dot(a[rows, :], wv_[:, lo : lo + COLS]).astype(bf16)
-        send(pb.at[his(d)], xb.at[d], s_.at[n], r_.at[n], sib)
-
-    def rs_first(a, wv_, pb, xb, fs, fr, gs, gr, s_, r_, prepare):
-        rs_rows(0, yo_y, a, wv_, pb, xb, s_, r_, prepare)
-        rs_rows(1, yn_y, a, wv_, pb, xb, s_, r_, prepare)
-        got(xb.at[yo_y], r_.at[0], "w_x0")
-        tot = pb[own(yo_y), :].astype(f32) + xb[yo_y].astype(f32)
-        fs[0] = tot[:, :COLS].astype(bf16)
-        fs[1] = tot[:, COLS:].astype(bf16)
-        send(fs.at[0], fr.at[0], s_.at[4], r_.at[4], yn)
-        send(fs.at[1], fr.at[1], s_.at[5], r_.at[5], yp)
-
-    def rs_second(a, wv_, pb, xb, fs, fr, gs, gr, s_, r_, prepare):
-        rs_rows(2, yp_y, a, wv_, pb, xb, s_, r_, prepare)
-        rs_rows(3, y, a, wv_, pb, xb, s_, r_, prepare)
-        got(xb.at[yn_y], r_.at[1], "w_x1")
-        tot = pb[own(yn_y), COLS:].astype(f32) + xb[yn_y, :, COLS:].astype(f32)
-        gs[1] = tot.astype(bf16)
-        send(gs.at[1], gr.at[1], s_.at[7], r_.at[7], yn)
-        got(xb.at[yp_y], r_.at[2], "w_x2")
-        tot = pb[own(yp_y), :COLS].astype(f32) + xb[yp_y, :, :COLS].astype(f32)
-        gs[2] = tot.astype(bf16)
-        send(gs.at[2], gr.at[2], s_.at[8], r_.at[8], yp)
-
-    def rs_mid(a, wv_, pb, xb, fs, fr, gs, gr, s_, r_):
-        got(fr.at[0], r_.at[4], "w_f0")
-        tot = pb[own(yn_y), :COLS].astype(f32) + xb[yn_y, :, :COLS].astype(f32)
-        gs[0] = (tot + fr[0].astype(f32)).astype(bf16)
-        send(gs.at[0], gr.at[0], s_.at[6], r_.at[6], yn)
-        got(fr.at[1], r_.at[5], "w_f1")
-        tot = pb[own(yp_y), COLS:].astype(f32) + xb[yp_y, :, COLS:].astype(f32)
-        gs[3] = (tot + fr[1].astype(f32)).astype(bf16)
-        send(gs.at[3], gr.at[3], s_.at[9], r_.at[9], yp)
-
-    def here(pb, xb, cs):
-        return pb[own(y), cs].astype(f32) + xb[y, :, cs].astype(f32)
-
-    def filtered(n, d):
-        @pl.when(jnp.logical_and(d == 0, sp > 0))
-        def _():
-            with scope("w_edge"):
-                edge.wait_recv()
-            prod[0:8, :] = er[8:16, :].astype(f32)
-
-        rows = pl.ds(pl.multiple_of(d * 192, 64), 192)
-        mine = pl.ds(pl.multiple_of(me * CH, CH), CH)
-        near = prod[pl.ds(pl.multiple_of(d * 192, 64), 200), :]
-        f = taps[0:1, mine] * near[6:198]
-        f = f + taps[1:2, mine] * near[7:199]
-        f = f + taps[2:3, mine] * near[8:200]
-        cbr[rows, :] = (proj[rows, 1024:1280].astype(f32) * f).astype(bf16)
-
-    conv_set = (cbr, woc_v, pb_c, x_c, fs_c, fr_c, gs_c, gr_c, rc_s, rc_r)
-    head_set = (mob, wom_v, pb_h, x_h, fs_h, fr_h, gs_h, gr_h, rh_s, rh_r)
-    weights[6].wait()
-    weights[7].wait()
     def start_carry(g, p):
         lo, hi = groups[g]
         n = TILES // (hi - lo)
@@ -489,7 +492,7 @@
             tiles = []
             for k in range(n):
                 p = (sp - lo) * n + k
-                r_i = pl.ds(pl.multiple_of((p // 2) * 8, 8), 8)
+                r_i = pl.ds(pl.multiple_of((p // 2) * 16, 16), 16)
                 c_i = pl.ds(pl.multiple_of(lax.rem(p, 2) * 128, 128), 128)
                 tiles.append(fmem[r_i, c_i])
             run_m = jnp.zeros((1, 128), f32)
@@ -497,7 +500,7 @@
         last_one = hi == n_sp
         for b in range(lo, hi):
             for k in range(n):
-                cv[b - lo, k] = tiles[k]
+                cv[b - lo, k] = tiles[k].astype(bf16)
             mh[b - lo] = run_m
             nh[b - lo] = run_n
             if b < hi - 1 or not last_one:
@@ -505,7 +508,7 @@
                 new_m = jnp.maximum(run_m + row[:, 0:128], row[:, 128:256])
                 old = jnp.exp(run_m + row[:, 0:128] - new_m)
                 new = jnp.exp(row[:, 128:256] - new_m)
-                tiles = [old * tiles[k] + new * rv[b - lo, k] for k in range(n)]
+                tiles = [old * tiles[k] + new * rv[b - lo, k].astype(f32) for k in range(n)]
                 run_n = old * run_n + new * row[:, 256:384]
                 run_m = new_m
         if not last_one:
@@ -529,18 +532,28 @@
             recurrence(g)
 
     with scope("rs_first_conv"):
-        rs_first(*conv_set, filtered)
-    take(0)
-    with scope("rs_second_conv"):
-        rs_second(*conv_set, filtered)
-
-    with scope("mixing"):
+        conv_part(0)
+        conv_part(3)
+        weights[6].wait()
+        weights[7].wait()
+        got(woc_v.at[pl.ds(CH, CH), :], ow_r.at[0])
+        got(wom_v.at[pl.ds(VAL, VAL), :], ow_r.at[1])
         top = jnp.broadcast_to(u_row, (8, BLK))
         urow[...] = top
         for s in (1, 2, 4, 8, 16, 32, 64, 128, 256, 512):
             top = jnp.maximum(top, jnp.where(lane >= s, pltpu.roll(top, s, 1), -jnp.inf))
         cols = jnp.concatenate([top, jnp.zeros((120, BLK), f32)], axis=0).T
         cmcol[...] = jnp.broadcast_to(cols[:, 0:1], (BLK, 128))
+        rs_first(*conv_set)
+    for g in range(len(groups)):
+        if g + 1 < len(groups):
+            take(g)
+
+            @pl.when(in_group(g))
+            def _():
+                conv_part(2, False)
+
+    with scope("mixing"):
         for rb in range(3):
             r0 = rb * 256
             q = proj[r0 : r0 + 256, 128:256]
@@ -560,8 +573,20 @@
             pv[r0 : r0 + 256, :] = acc
             rs[r0 : r0 + 256, :] = jnp.broadcast_to(tot, (256, 128))
 
-    for g in range(1, len(groups)):
-        take(g)
+    with scope("rs_second_conv"):
+
+        @pl.when(in_group(len(groups) - 1))
+        def _():
+            conv_part(2, False)
+
+        sends.append(
+            pltpu.make_async_remote_copy(
+                src_ref=cbr.at[his(order[2])], dst_ref=x_c.at[2], send_sem=rc_s.at[2],
+                recv_sem=rc_r.at[2], device_id=(sp, sib), device_id_type=MESH,
+            )
+        )
+        rs_second(*conv_set)
+    take(len(groups) - 1)
     with scope("rs_mid_conv"):
         rs_mid(*conv_set)
 
@@ -574,10 +599,8 @@
     with scope("carry"):
         for p in range(TILES):
             i, j = p // 2, p % 2
-            cmem[8 * i : 8 * i + 8, 128 * j : 128 * j + 128] = cr[p]
+            cmem[16 * i : 16 * i + 16, 128 * j : 128 * j + 128] = cr[p]
         carry = cmem[...]
-        high = carry.astype(bf16)
-        low = (carry - high.astype(f32)).astype(bf16)
         m_in = m_at[:, 0:1]
         n_in = n_at[...]
         n_1 = n_in.astype(bf16).astype(f32)
@@ -595,7 +618,7 @@
         peak = jnp.maximum(cm, m_in)
         f_in = jnp.exp(cm - peak)
         f_carry = jnp.exp(m_in - peak)
-        from_memory = (dot(q, high) + dot(q, low)) * SCALE
+        from_memory = dot(q, carry) * SCALE
         from_norm = jnp.sum(nt_dot(q, n_rows), axis=1, keepdims=True) * SCALE
         num = f_in * pv[rows, :] + f_carry * from_memory
         den = f_in * rs[rows, 0:1] + f_carry * from_norm
@@ -605,9 +628,12 @@
         mob[rows, :] = memory_out.astype(bf16)
 
     with scope("rs_first_head"):
-        rs_first(*head_set, heads)
+        for n in (0, 1, 2):
+            rs_part(n, mob, wom_v, x_h, rh_s, rh_r, heads)
+        rs_first(*head_set)
     with scope("rs_second_head"):
-        rs_second(*head_set, heads)
+        rs_part(3, mob, wom_v, x_h, rh_s, rh_r, heads)
+        rs_second(*head_set)
     ss[me] = sqcol[...].T[0:1]
     for k in range(1, NTP):
         send(ss.at[me], ss.at[me], ss_s.at[k], ss_r.at[k], lax.rem(me + k, NTP))
@@ -620,22 +646,20 @@
         total = total + ss[k]
     factor = lax.rsqrt(total / (NTP * VAL) + EPS)
     scol[...] = jnp.broadcast_to(factor, (128, BLK)).T
-    got(x_c.at[y], rc_r.at[3])
     for k in range(4):
         got(gr_c.at[k], rc_r.at[6 + k], "w_gc")
-    got(x_h.at[y], rh_r.at[3])
     factor = scol[pl.ds(pl.multiple_of(me * ROWS, 8), ROWS), 0:1]
     for k in range(2):
         cs = slice(k * COLS, (k + 1) * COLS)
-        conv_sum = here(pb_c, x_c, cs) + gr_c[k].astype(f32) + gr_c[2 + k].astype(f32)
-        fin[:, cs] = conv_sum + factor * here(pb_h, x_h, cs)
+        conv_sum = own_c[:, cs] + gr_c[k].astype(f32) + gr_c[2 + k].astype(f32)
+        own_c[:, cs] = conv_sum + factor * own_h[:, cs]
     for k in (1, 2, 0, 3):
         got(gr_h.at[k], rh_r.at[6 + k], "w_gh")
     with scope("final"):
         for k in range(2):
             cs = slice(k * COLS, (k + 1) * COLS)
             rest_sum = gr_h[k].astype(f32) + gr_h[2 + k].astype(f32)
-            out[:, cs] = (fin[:, cs] + factor * rest_sum).astype(bf16)
+            out[:, cs] = (own_c[:, cs] + factor * rest_sum).astype(bf16)
 
     for cp in sends:
         cp.wait_send()
@@ -673,8 +697,7 @@
 
     def rs_bufs():
         return [
-            pltpu.VMEM((BLK, D), bf16),
-            pltpu.VMEM((4, ROWS, D), bf16),
+            pltpu.VMEM((4, ROWS, CH), bf16),
             pltpu.VMEM((2, ROWS, COLS), bf16),
             pltpu.VMEM((2, ROWS, COLS), bf16),
             pltpu.VMEM((4, ROWS, COLS), bf16),
@@ -693,26 +716,26 @@
         pltpu.VMEM((1, KEY), f32),
         pltpu.VMEM((BLK, D), bf16),
         pltpu.VMEM((D, 1408), bf16),
-        pltpu.VMEM((VAL, D), bf16),
-        pltpu.VMEM((CH, D), bf16),
+        pltpu.VMEM((2 * VAL, D), bf16),
+        pltpu.VMEM((2 * CH, D), bf16),
         pltpu.VMEM((BLK, 1280), bf16),
         pltpu.VMEM((BLK, 128), f32),
         pltpu.VMEM((8, BLK), f32),
         pltpu.VMEM((BLK, 128), f32),
-        pltpu.VMEM((TILES, 8, 128), f32),
-        pltpu.VMEM((gmax, tmax, 8, 128), f32),
+        pltpu.VMEM((TILES, 16, 128), bf16),
+        pltpu.VMEM((gmax, tmax, 16, 128), bf16),
         pltpu.VMEM((n_sp, 1, 384), f32),
-        pltpu.VMEM((gmax, tmax, 8, 128), f32),
-        pltpu.VMEM((TILES, 8, 128), f32),
+        pltpu.VMEM((gmax, tmax, 16, 128), bf16),
+        pltpu.VMEM((TILES, 16, 128), bf16),
         pltpu.VMEM((gmax, 1, 128), f32),
         pltpu.VMEM((gmax, 1, 128), f32),
         pltpu.VMEM((1, 128), f32),
         pltpu.VMEM((1, 128), f32),
-        pltpu.VMEM((tmax, 8, 128), f32),
+        pltpu.VMEM((tmax, 16, 128), f32),
         pltpu.VMEM((1, 256), f32),
-        pltpu.VMEM((tmax, 8, 128), f32),
+        pltpu.VMEM((tmax, 16, 128), f32),
         pltpu.VMEM((1, 256), f32),
-        pltpu.VMEM((KEY, VAL), f32),
+        pltpu.VMEM((KEY, VAL), bf16),
         pltpu.VMEM((BLK, VAL), f32),
         pltpu.VMEM((BLK, 128), f32),
         pltpu.VMEM((BLK, VAL), bf16),
@@ -724,6 +747,8 @@
         pltpu.VMEM((BLK, 128), f32),
         pltpu.VMEM((BLK, 128), f32),
         pltpu.VMEM((ROWS, D), f32),
+        pltpu.VMEM((ROWS, D), f32),
+        pltpu.VMEM((2, ROWS, COLS), f32),
         *rs_bufs(),
         *rs_bufs(),
         dma((8,)),
@@ -750,6 +775,8 @@
         dma(()),
         pltpu.SemaphoreType.REGULAR,
         pltpu.SemaphoreType.REGULAR,
+        dma((2,)),
+        dma((2,)),
     ]
 
     def per_device(

time: 60.3 us -> 57.8 us (0.959)
  the two profiles are of different devices: /device:TPU:129 before, /device:TPU:1 now
where the time goes in v4:
time: 57.8 us; the launch traced here: 57.6 us
  Pallas kernels  55.9 us (97%)
  local copies, waits for them, and re-layouts  1.77 us (3%)
    pallas_call x1, Pallas kernels, per_device(): pl.pallas_call(functools.partial(kernel, n_sp), out_shape=jax.ShapeDtypeS...  55.9 us
    unnamed x1, local copies, waits for them, and re-layouts  1.77 us

profile of v4, /device:TPU:1, one launch (start us, length us, event | category | flops | bytes accessed | tf_op | source)
XLA Modules:
  0.0 57.6 jit_solution(17050884773580406135)
XLA Ops:
  0.0 55.9 %shard_map.163 = bf16[96,2048]{1,0:T(8,128)(2,1)} custom-call(bf16[96,2048]{1,0:T(8,128)(2,1)} %tok_h.1, f32[1,2048]{1,0:T(1,128)} %bitcast.9, bf16[8,2048]{1,0:T(8,128)(2,1)} %bitcast.7, bf16[8,2048]{1,0:T(8,128)(2,1)} %bitcast.8, f32[1,8]{1,0:T(1,128)} %bitcast.11, f32[1,768]{1,0:T(1,128)} %bitcast.10, f32[3,2048]{1,0:T(4,128)} %taps_h.1, ...), custom_call_target="tpu_custom_call" | custom-call | tf_op jit(solution)/shard_map/pallas_call | solution.py:787
  55.9 1.8 %copy.19 = bf16[96,2048]{1,0:T(8,128)(2,1)} copy(bf16[96,2048]{1,0:T(8,128)(2,1)} %shard_map.163) | data formatting | bytes 786432

commit v5 on v4

--- a/solution.py
+++ b/solution.py
@@ -17,6 +17,7 @@
 NTP = 8
 TILES = 16
 COLS = 1024
+AG_SLOT = (0, 1, 2, 3, 4, 5, 6, 7, 7, 8, 8, 9, 9)
 EPS = 1e-06
 SCALE = KEY ** (-0.5)
 MESH = pl.DeviceIdType.MESH
@@ -44,16 +45,16 @@
     n_sp,
     tok_h, gain_h, wi_h, wf_h, bias_h, fextra_h, taps_h, fmem_h, fnorm_h,
     wq, wk, wv, wcg, wcl, wcr, wom, woc,
-    out,
+    out_h,
     tok, gain, wi, wf, bias, fextra, taps, fmem, fnorm,
     x, w_all, wom_v, woc_v,
     proj, gates, urow, cmcol, st, rv, aux, cv, cr, mh, nh, m_at, n_at,
     ex, ea, px, pa, cmem, pv, rs,
-    mob, cbr, prod, eb, er, ss, scol, sqcol, own_c, own_h, part,
+    mob, cbr, prod, eb, er, ss, scol, sqcol, own_c, own_h, part, out,
     x_c, fs_c, fr_c, gs_c, gr_c,
     x_h, fs_h, fr_h, gs_h, gr_h,
     wsem, isem, ag_s, ag_r, aux_s, aux_r, st_s, st_r, cr_s, cr_r, ed_s, ed_r, ss_s, ss_r,
-    rc_s, rc_r, rh_s, rh_r, ex_s, px_r, ea_s, pa_r, ready, ready_edge, ow_s, ow_r,
+    rc_s, rc_r, rh_s, rh_r, ex_s, px_r, ea_s, pa_r, ready, ready_edge, ow_s, ow_r, out_s,
 ):
     groups = groups_of(n_sp)
     scope = jax.named_scope
@@ -98,7 +99,7 @@
         )
     ]
     weights = [
-        pltpu.make_async_copy(src, dst, wsem.at[i])
+        pltpu.make_async_copy(src, dst, wsem.at[i // 6])
         for i, (src, dst) in enumerate(
             [
                 (wk, w_all.at[:, pl.ds(0, 128)]),
@@ -167,15 +168,12 @@
                 def _(count=count):
                     pl.semaphore_wait(barrier, count + 1)
 
-    sends = []
-
     def send(src, dst, ssem, rsem, peer):
         cp = pltpu.make_async_remote_copy(
             src_ref=src, dst_ref=dst, send_sem=ssem, recv_sem=rsem,
             device_id=(sp, peer), device_id_type=MESH,
         )
         cp.start()
-        sends.append(cp)
 
     def got(dst, rsem, name="w"):
         with scope(name):
@@ -185,7 +183,7 @@
             ).wait_recv()
 
     def ag(src, dst, k, peer, n=1):
-        send(slots(src, n), slots(dst, n), ag_s.at[k], ag_r.at[k], peer)
+        send(slots(src, n), slots(dst, n), ag_s, ag_r.at[AG_SLOT[k]], peer)
 
     other = 1 - c
     ag(2 * c, 4 + c, 0, yn)
@@ -193,8 +191,8 @@
     ag(2 * c + 1, 8 + c, 1, yn)
     ag(2 * c, 10 + c, 4, yp)
     ag(2 * c, 2 * c, 6, sib, 2)
-    send(woc, woc_v.at[pl.ds(CH, CH), :], ow_s.at[0], ow_r.at[0], sib)
-    send(wom, wom_v.at[pl.ds(VAL, VAL), :], ow_s.at[1], ow_r.at[1], sib)
+    send(woc, woc_v.at[pl.ds(CH, CH), :], ow_s, ow_r, sib)
+    send(wom, wom_v.at[pl.ds(VAL, VAL), :], ow_s, ow_r, sib)
     def tell(sem, p):
         pl.semaphore_signal(sem, inc=1, device_id=(p, me), device_id_type=MESH)
 
@@ -216,20 +214,18 @@
     )
     w_all[:, 1280:1408] = gw.T.astype(bf16)
     with scope("w_weights"):
-        for i in range(6):
-            weights[i].wait()
-
-    def project(stage, bases, parts):
-        xs = x[stage * 192 : stage * 192 + 192, :]
+        pltpu.make_async_copy(w_all.at[:, 0:1280], w_all.at[:, 0:1280], wsem.at[0]).wait()
+
+    def project_rows(xs, bases, n, parts):
         for lo, hi in parts:
             res = dot(xs, w_all[:, lo:hi])
             for k, base in enumerate(bases):
-                rows = pl.ds(pl.multiple_of(base, 16), HALF)
-                piece = res[k * HALF : (k + 1) * HALF]
+                rows = pl.ds(pl.multiple_of(base, 16), n)
+                piece = res[k * n : (k + 1) * n]
                 if lo == 512:
                     left = piece[:, :CH].astype(bf16).astype(f32)
                     right = piece[:, CH:].astype(bf16).astype(f32)
-                    at = pl.ds(pl.multiple_of(base + 8, 8), HALF)
+                    at = pl.ds(pl.multiple_of(base + 8, 8), n)
                     prod[at, :] = (left * right).astype(bf16).astype(f32)
                 elif hi <= 1280:
                     proj[rows, lo:hi] = piece.astype(bf16)
@@ -238,6 +234,9 @@
                     if lo < 1280:
                         proj[rows, lo:1280] = piece[:, : 1280 - lo].astype(bf16)
 
+    def project(stage, bases, parts):
+        project_rows(x[stage * 192 : stage * 192 + 192, :], bases, HALF, parts)
+
     edge = pltpu.make_async_remote_copy(
         src_ref=eb, dst_ref=er, send_sem=ed_s, recv_sem=ed_r,
         device_id=(lax.rem(sp + 1, n_sp), me), device_id_type=MESH,
@@ -263,11 +262,10 @@
 
     order = (yo_y, yn_y, yp_y, y)
 
-    def rs_part(n, a, w, xb, s_, r_, prepare, kept=True):
-        prepare(n, order[n])
-        send(a.at[his(order[n])], xb.at[n], s_.at[n], r_.at[n], sib)
-        if not kept:
-            sends.pop()
+    def rs_part(n, a, w, xb, s_, r_, prepare):
+        prepare(order[n], other)
+        send(a.at[his(order[n])], xb.at[n], s_, r_.at[0 if n == 0 else 1], sib)
+        prepare(order[n], c)
 
     def both(n, a, xb):
         return jnp.concatenate([a[own(order[n]), :], xb[n]], axis=1)
@@ -277,51 +275,51 @@
         lhs = both(0, a, xb)
         for k, peer in ((0, yn), (1, yp)):
             fs[k] = dot(lhs, w[:, k * COLS : (k + 1) * COLS]).astype(bf16)
-            send(fs.at[k], fr.at[k], s_.at[4 + k], r_.at[4 + k], peer)
+            send(fs.at[k], fr.at[k], s_, r_.at[2 + k], peer)
 
     def rs_second(a, w, xb, fs, fr, gs, gr, kept, s_, r_):
-        for n in (1, 2, 3):
-            got(xb.at[n], r_.at[n], "w_x123")
+        got(xb.at[pl.ds(1, 3)], r_.at[1], "w_x123")
         lhs = jnp.concatenate([both(n, a, xb) for n in (1, 2, 3)], axis=0)
         res = dot(lhs, w[:, COLS:])
         gs[1] = res[0:ROWS].astype(bf16)
-        send(gs.at[1], gr.at[1], s_.at[7], r_.at[7], yn)
+        send(gs.at[1], gr.at[1], s_, r_.at[4], yn)
         part[1] = res[ROWS : 2 * ROWS]
         kept[:, COLS:] = res[2 * ROWS :]
         res = dot(lhs, w[:, :COLS])
         gs[2] = res[ROWS : 2 * ROWS].astype(bf16)
-        send(gs.at[2], gr.at[2], s_.at[8], r_.at[8], yp)
+        send(gs.at[2], gr.at[2], s_, r_.at[4], yp)
         part[0] = res[0:ROWS]
         kept[:, :COLS] = res[2 * ROWS :]
 
     def rs_mid(a, w, xb, fs, fr, gs, gr, kept, s_, r_):
-        got(fr.at[0], r_.at[4], "w_f0")
+        got(fr.at[0], r_.at[2], "w_f0")
         gs[0] = (part[0] + fr[0].astype(f32)).astype(bf16)
-        send(gs.at[0], gr.at[0], s_.at[6], r_.at[6], yn)
-        got(fr.at[1], r_.at[5], "w_f1")
+        send(gs.at[0], gr.at[0], s_, r_.at[4], yn)
+        got(fr.at[1], r_.at[3], "w_f1")
         gs[3] = (part[1] + fr[1].astype(f32)).astype(bf16)
-        send(gs.at[3], gr.at[3], s_.at[9], r_.at[9], yp)
-
-    def filtered(n, d):
-        @pl.when(jnp.logical_and(d == 0, sp > 0))
+        send(gs.at[3], gr.at[3], s_, r_.at[4], yp)
+
+    def filtered(d, core):
+        @pl.when(jnp.logical_and(jnp.logical_and(d == 0, core == 0), sp > 0))
         def _():
             with scope("w_edge"):
                 edge.wait_recv()
             prod[0:8, :] = er[8:16, :].astype(f32)
 
-        rows = pl.ds(pl.multiple_of(d * 192, 64), 192)
+        at = (d * 2 + core) * ROWS
+        rows = pl.ds(pl.multiple_of(at, 16), ROWS)
         mine = pl.ds(pl.multiple_of(me * CH, CH), CH)
-        near = prod[pl.ds(pl.multiple_of(d * 192, 64), 200), :]
-        f = taps[0:1, mine] * near[6:198]
-        f = f + taps[1:2, mine] * near[7:199]
-        f = f + taps[2:3, mine] * near[8:200]
+        near = prod[pl.ds(pl.multiple_of(at, 16), ROWS + 8), :]
+        f = taps[0:1, mine] * near[6 : 6 + ROWS]
+        f = f + taps[1:2, mine] * near[7 : 7 + ROWS]
+        f = f + taps[2:3, mine] * near[8 : 8 + ROWS]
         cbr[rows, :] = (proj[rows, 1024:1280].astype(f32) * f).astype(bf16)
 
     conv_set = (cbr, woc_v, x_c, fs_c, fr_c, gs_c, gr_c, own_c, rc_s, rc_r)
     head_set = (mob, wom_v, x_h, fs_h, fr_h, gs_h, gr_h, own_h, rh_s, rh_r)
 
-    def conv_part(n, kept=True):
-        rs_part(n, cbr, woc_v, x_c, rc_s, rc_r, filtered, kept)
+    def conv_part(n):
+        rs_part(n, cbr, woc_v, x_c, rc_s, rc_r, filtered)
 
     every = ((0, 512), (512, 1024), (1024, 1408))
     got(slots(2 * other, 2), ag_r.at[6], "w_ag6")
@@ -329,13 +327,12 @@
         project(0, [y * 192 + HALF * k for k in range(4)], every)
         send_edge(3)
     got(slots(4 + c), ag_r.at[0], "w_ag0")
-    ag(4 + c, 12 + c, 2, yn)
+    ag(4 + c, 12 + 2 * c, 2, yn)
     ag(4 + c, 4 + c, 7, sib)
     got(slots(6 + c), ag_r.at[3], "w_ag3")
-    ag(6 + c, 14 + c, 5, yp)
+    ag(6 + c, 13 + 2 * c, 5, yp)
     ag(6 + c, 6 + c, 8, sib)
-    got(slots(4 + other), ag_r.at[7], "w_ag7")
-    got(slots(6 + other), ag_r.at[8], "w_ag8")
+    got(slots(0, 2), ag_r.at[7], "w_ag7")
     with scope("proj_1"):
         project(
             1,
@@ -347,8 +344,7 @@
     ag(8 + c, 8 + c, 9, sib)
     got(slots(10 + c), ag_r.at[4], "w_ag4")
     ag(10 + c, 10 + c, 10, sib)
-    got(slots(8 + other), ag_r.at[9], "w_ag9")
-    got(slots(10 + other), ag_r.at[10], "w_ag10")
+    got(slots(0, 2), ag_r.at[8], "w_ag9")
     with scope("proj_2"):
         project(
             2,
@@ -356,17 +352,23 @@
             every,
         )
         send_edge(0)
-    got(slots(12 + c), ag_r.at[2], "w_ag2")
-    ag(12 + c, 12 + c, 11, sib)
-    got(slots(14 + c), ag_r.at[5], "w_ag5")
-    ag(14 + c, 14 + c, 12, sib)
+    got(slots(12 + 2 * c), ag_r.at[2], "w_ag2")
+    ag(12 + 2 * c, 12 + 2 * c, 11, sib)
+    got(slots(13 + 2 * c), ag_r.at[5], "w_ag5")
+    ag(13 + 2 * c, 13 + 2 * c, 12, sib)
     with scope("conv_early"):
         conv_part(1)
-    got(slots(12 + other), ag_r.at[11], "w_ag11")
-    got(slots(14 + other), ag_r.at[12], "w_ag12")
-    last = [yo_y * 192, yo_y * 192 + ROWS, yo_y * 192 + HALF, yo_y * 192 + ROWS + HALF]
+    keys, rest = ((1280, 1408), (0, 512)), ((512, 1024), (1024, 1280))
+
+    def project_last(core, parts):
+        xs = x[pl.ds(pl.multiple_of(576 + core * ROWS, 16), ROWS), :]
+        project_rows(xs, [yo_y * 192 + core * ROWS], ROWS, parts)
+
+    with scope("proj_3own"):
+        project_last(c, keys + rest)
+    got(slots(0, 2), ag_r.at[9], "w_ag12")
     with scope("proj_3"):
-        project(3, last, ((1280, 1408), (0, 512)))
+        project_last(other, keys)
 
     with scope("state"):
         g_t = gates[...].T
@@ -445,9 +447,8 @@
                     rv[sp - lo, k] = st[(sp - lo) * n + k]
 
     with scope("proj_lrg"):
-        project(3, last, ((512, 1024),))
+        project_last(other, rest)
         send_edge(1)
-        project(3, last, ((1024, 1280),))
 
     def start_carry(g, p):
         lo, hi = groups[g]
@@ -534,10 +535,8 @@
     with scope("rs_first_conv"):
         conv_part(0)
         conv_part(3)
-        weights[6].wait()
-        weights[7].wait()
-        got(woc_v.at[pl.ds(CH, CH), :], ow_r.at[0])
-        got(wom_v.at[pl.ds(VAL, VAL), :], ow_r.at[1])
+        pltpu.make_async_copy(woc_v, woc_v, wsem.at[1]).wait()
+        got(woc_v, ow_r)
         top = jnp.broadcast_to(u_row, (8, BLK))
         urow[...] = top
         for s in (1, 2, 4, 8, 16, 32, 64, 128, 256, 512):
@@ -545,15 +544,7 @@
         cols = jnp.concatenate([top, jnp.zeros((120, BLK), f32)], axis=0).T
         cmcol[...] = jnp.broadcast_to(cols[:, 0:1], (BLK, 128))
         rs_first(*conv_set)
-    for g in range(len(groups)):
-        if g + 1 < len(groups):
-            take(g)
-
-            @pl.when(in_group(g))
-            def _():
-                conv_part(2, False)
-
-    with scope("mixing"):
+    def mixing():
         for rb in range(3):
             r0 = rb * 256
             q = proj[r0 : r0 + 256, 128:256]
@@ -573,19 +564,24 @@
             pv[r0 : r0 + 256, :] = acc
             rs[r0 : r0 + 256, :] = jnp.broadcast_to(tot, (256, 128))
 
+    last_group = in_group(len(groups) - 1)
+    for g in range(len(groups) - 1):
+        take(g)
+
+    @pl.when(last_group)
+    def _():
+        with scope("mixing"):
+            mixing()
+
     with scope("rs_second_conv"):
-
-        @pl.when(in_group(len(groups) - 1))
-        def _():
-            conv_part(2, False)
-
-        sends.append(
-            pltpu.make_async_remote_copy(
-                src_ref=cbr.at[his(order[2])], dst_ref=x_c.at[2], send_sem=rc_s.at[2],
-                recv_sem=rc_r.at[2], device_id=(sp, sib), device_id_type=MESH,
-            )
-        )
+        conv_part(2)
         rs_second(*conv_set)
+
+    @pl.when(jnp.logical_not(last_group))
+    def _():
+        with scope("mixing"):
+            mixing()
+
     take(len(groups) - 1)
     with scope("rs_mid_conv"):
         rs_mid(*conv_set)
@@ -611,8 +607,8 @@
             sub16 == 0, n_1, jnp.where(sub16 == 1, n_2, jnp.where(sub16 == 2, n_3, 0.0))
         ).astype(bf16)
 
-    def heads(n, d):
-        rows = pl.ds(pl.multiple_of(d * 192, 64), 192)
+    def heads(d, core):
+        rows = pl.ds(pl.multiple_of((d * 2 + core) * ROWS, 16), ROWS)
         q = proj[rows, 128:256]
         cm = cmcol[rows, 0:1]
         peak = jnp.maximum(cm, m_in)
@@ -624,7 +620,7 @@
         den = f_in * rs[rows, 0:1] + f_carry * from_norm
         memory_out = num / jnp.maximum(jnp.abs(den), 1.0)
         squares = jnp.sum(memory_out * memory_out, axis=1, keepdims=True)
-        sqcol[rows, :] = jnp.broadcast_to(squares, (192, 128))
+        sqcol[rows, :] = jnp.broadcast_to(squares, (ROWS, 128))
         mob[rows, :] = memory_out.astype(bf16)
 
     with scope("rs_first_head"):
@@ -636,38 +632,43 @@
         rs_second(*head_set)
     ss[me] = sqcol[...].T[0:1]
     for k in range(1, NTP):
-        send(ss.at[me], ss.at[me], ss_s.at[k], ss_r.at[k], lax.rem(me + k, NTP))
+        send(ss.at[me], ss.at[me], ss_s, ss_r, lax.rem(me + k, NTP))
     with scope("rs_mid_head"):
         rs_mid(*head_set)
-    for k in range(1, NTP):
-        got(ss.at[lax.rem(me + NTP - k, NTP)], ss_r.at[k], "w_ss")
+    got(ss.at[pl.ds(0, NTP - 1)], ss_r, "w_ss")
     total = ss[0]
     for k in range(1, NTP):
         total = total + ss[k]
     factor = lax.rsqrt(total / (NTP * VAL) + EPS)
     scol[...] = jnp.broadcast_to(factor, (128, BLK)).T
-    for k in range(4):
-        got(gr_c.at[k], rc_r.at[6 + k], "w_gc")
+    got(gr_c, rc_r.at[4], "w_gc")
     factor = scol[pl.ds(pl.multiple_of(me * ROWS, 8), ROWS), 0:1]
     for k in range(2):
         cs = slice(k * COLS, (k + 1) * COLS)
         conv_sum = own_c[:, cs] + gr_c[k].astype(f32) + gr_c[2 + k].astype(f32)
         own_c[:, cs] = conv_sum + factor * own_h[:, cs]
-    for k in (1, 2, 0, 3):
-        got(gr_h.at[k], rh_r.at[6 + k], "w_gh")
+    got(gr_h, rh_r.at[4], "w_gh")
+    outs = []
     with scope("final"):
         for k in range(2):
             cs = slice(k * COLS, (k + 1) * COLS)
             rest_sum = gr_h[k].astype(f32) + gr_h[2 + k].astype(f32)
             out[:, cs] = (own_c[:, cs] + factor * rest_sum).astype(bf16)
-
-    for cp in sends:
-        cp.wait_send()
+            outs.append(pltpu.make_async_copy(out.at[:, cs], out_h.at[:, cs], out_s.at[k]))
+            outs[k].start()
+
     def sent(ref, sem):
         pltpu.make_async_remote_copy(
             src_ref=ref, dst_ref=ref, send_sem=sem, recv_sem=sem,
             device_id=(sp, sib), device_id_type=MESH,
         ).wait_send()
+
+    with scope("w_sends"):
+        sent(x.at[pl.ds(0, 14 * HALF), :], ag_s)
+        sent(woc_v, ow_s)
+        sent(x.at[pl.ds(0, 336), :], rc_s)
+        sent(x.at[pl.ds(0, 336), :], rh_s)
+        sent(ss.at[pl.ds(0, NTP - 1)], ss_s)
 
     @pl.when(sp < n_sp - 1)
     def _():
@@ -685,13 +686,16 @@
             for cp in pass_on(g):
                 cp.wait_send()
 
+    with scope("w_out"):
+        for cp in outs:
+            cp.wait()
+
 
 def solution(mesh):
     n_sp = mesh.shape["sp"]
     groups = groups_of(n_sp)
     gmax = max(hi - lo for lo, hi in groups)
     tmax = max(TILES // (hi - lo) for lo, hi in groups)
-    vmem = pl.BlockSpec(memory_space=pltpu.VMEM)
     hbm = pl.BlockSpec(memory_space=pl.ANY)
     dma = pltpu.SemaphoreType.DMA
 
@@ -749,33 +753,28 @@
         pltpu.VMEM((ROWS, D), f32),
         pltpu.VMEM((ROWS, D), f32),
         pltpu.VMEM((2, ROWS, COLS), f32),
+        pltpu.VMEM((ROWS, D), bf16),
         *rs_bufs(),
         *rs_bufs(),
-        dma((8,)),
+        dma((2,)),
         dma((9,)),
-        dma((13,)),
-        dma((13,)),
+        dma(()),
+        dma((10,)),
+        *[dma(()) for _ in range(8)],
         dma(()),
         dma(()),
         dma(()),
+        dma((5,)),
         dma(()),
+        dma((5,)),
+        dma((2,)),
         dma(()),
-        dma(()),
-        dma(()),
-        dma(()),
-        dma((NTP,)),
-        dma((NTP,)),
-        dma((10,)),
-        dma((10,)),
-        dma((10,)),
-        dma((10,)),
-        dma((4,)),
-        dma(()),
-        dma((4,)),
+        dma((2,)),
         dma(()),
         pltpu.SemaphoreType.REGULAR,
         pltpu.SemaphoreType.REGULAR,
-        dma((2,)),
+        dma(()),
+        dma(()),
         dma((2,)),
     ]
 
@@ -788,7 +787,7 @@
             functools.partial(kernel, n_sp),
             out_shape=jax.ShapeDtypeStruct((ROWS, D), bf16),
             in_specs=[hbm] * 17,
-            out_specs=vmem,
+            out_specs=hbm,
             scratch_shapes=scratch,
             compiler_params=pltpu.CompilerParams(
                 collective_id=0, has_side_effects=True, vmem_limit_bytes=60 * 1024 * 1024

time: 57.8 us -> 57 us (0.986)
  Pallas kernels: 55.9 us -> 55.2 us
    pallas_call x1, Pallas kernels: 55.9 us -> 55.2 us  [per_device(): pl.pallas_call(functools.partial(kernel, n_sp), out_shape=jax.ShapeDtypeS...]
where the time goes in v5:
time: 57 us; the launch traced here: 56.9 us
  Pallas kernels  55.2 us (97%)
  local copies, waits for them, and re-layouts  1.77 us (3%)
    pallas_call x1, Pallas kernels, per_device(): pl.pallas_call(functools.partial(kernel, n_sp), out_shape=jax.ShapeDtypeS...  55.2 us
    unnamed x1, local copies, waits for them, and re-layouts  1.77 us

profile of v5, /device:TPU:1, one launch (start us, length us, event | category | flops | bytes accessed | tf_op | source)
XLA Modules:
  0.0 56.9 jit_solution(1595434737494050347)
XLA Ops:
  0.0 55.2 %shard_map.163 = bf16[96,2048]{1,0:T(8,128)(2,1)} custom-call(bf16[96,2048]{1,0:T(8,128)(2,1)} %tok_h.1, f32[1,2048]{1,0:T(1,128)} %bitcast.9, bf16[8,2048]{1,0:T(8,128)(2,1)} %bitcast.7, bf16[8,2048]{1,0:T(8,128)(2,1)} %bitcast.8, f32[1,8]{1,0:T(1,128)} %bitcast.11, f32[1,768]{1,0:T(1,128)} %bitcast.10, f32[3,2048]{1,0:T(4,128)} %taps_h.1, ...), custom_call_target="tpu_custom_call" | custom-call | tf_op jit(solution)/shard_map/pallas_call | solution.py:786
  55.2 1.8 %copy.19 = bf16[96,2048]{1,0:T(8,128)(2,1)} copy(bf16[96,2048]{1,0:T(8,128)(2,1)} %shard_map.163) | data formatting | bytes 786432

commit v6 on v5

--- a/solution.py
+++ b/solution.py
@@ -17,6 +17,7 @@
 NTP = 8
 TILES = 16
 COLS = 1024
+CUT = 1280
 AG_SLOT = (0, 1, 2, 3, 4, 5, 6, 7, 7, 8, 8, 9, 9)
 EPS = 1e-06
 SCALE = KEY ** (-0.5)
@@ -264,40 +265,46 @@
 
     def rs_part(n, a, w, xb, s_, r_, prepare):
         prepare(order[n], other)
-        send(a.at[his(order[n])], xb.at[n], s_, r_.at[0 if n == 0 else 1], sib)
+        send(a.at[his(order[n])], xb.at[n], s_, r_.at[(0, 5, 1, 1)[n]], sib)
         prepare(order[n], c)
 
     def both(n, a, xb):
         return jnp.concatenate([a[own(order[n]), :], xb[n]], axis=1)
 
-    def rs_first(a, w, xb, fs, fr, gs, gr, kept, s_, r_):
+    def rs_first(cut, a, w, xb, fs, fr, gs, gr, kept, s_, r_):
         got(xb.at[0], r_.at[0], "w_x0")
         lhs = both(0, a, xb)
-        for k, peer in ((0, yn), (1, yp)):
-            fs[k] = dot(lhs, w[:, k * COLS : (k + 1) * COLS]).astype(bf16)
-            send(fs.at[k], fr.at[k], s_, r_.at[2 + k], peer)
-
-    def rs_second(a, w, xb, fs, fr, gs, gr, kept, s_, r_):
-        got(xb.at[pl.ds(1, 3)], r_.at[1], "w_x123")
-        lhs = jnp.concatenate([both(n, a, xb) for n in (1, 2, 3)], axis=0)
-        res = dot(lhs, w[:, COLS:])
-        gs[1] = res[0:ROWS].astype(bf16)
-        send(gs.at[1], gr.at[1], s_, r_.at[4], yn)
-        part[1] = res[ROWS : 2 * ROWS]
-        kept[:, COLS:] = res[2 * ROWS :]
-        res = dot(lhs, w[:, :COLS])
-        gs[2] = res[ROWS : 2 * ROWS].astype(bf16)
-        send(gs.at[2], gr.at[2], s_, r_.at[4], yp)
-        part[0] = res[0:ROWS]
-        kept[:, :COLS] = res[2 * ROWS :]
-
-    def rs_mid(a, w, xb, fs, fr, gs, gr, kept, s_, r_):
-        got(fr.at[0], r_.at[2], "w_f0")
-        gs[0] = (part[0] + fr[0].astype(f32)).astype(bf16)
-        send(gs.at[0], gr.at[0], s_, r_.at[4], yn)
-        got(fr.at[1], r_.at[3], "w_f1")
-        gs[3] = (part[1] + fr[1].astype(f32)).astype(bf16)
-        send(gs.at[3], gr.at[3], s_, r_.at[4], yp)
+        for k, (lo, hi, peer) in enumerate(((0, cut, yn), (cut, D, yp))):
+            fs[:, lo:hi] = dot(lhs, w[:, lo:hi]).astype(bf16)
+            send(fs.at[:, lo:hi], fr.at[:, lo:hi], s_, r_.at[2 + k], peer)
+
+    def rs_early(cut, a, w, xb, fs, fr, gs, gr, kept, s_, r_):
+        got(xb.at[1], r_.at[5], "w_x1")
+        gs[0, :, cut:] = dot(both(1, a, xb), w[:, cut:]).astype(bf16)
+        send(gs.at[0, :, cut:], gr.at[0, :, cut:], s_, r_.at[4], yn)
+
+    def rs_second(early, cut, a, w, xb, fs, fr, gs, gr, kept, s_, r_):
+        if not early:
+            got(xb.at[1], r_.at[5], "w_x1")
+        got(xb.at[pl.ds(2, 2)], r_.at[1], "w_x23")
+        low = jnp.concatenate([both(n, a, xb) for n in (2, 3, 1)], axis=0)
+        res = dot(low[: 2 * ROWS] if early else low, w[:, cut:])
+        if not early:
+            gs[0, :, cut:] = res[2 * ROWS :].astype(bf16)
+            send(gs.at[0, :, cut:], gr.at[0, :, cut:], s_, r_.at[4], yn)
+        part[:, cut:] = res[0:ROWS]
+        kept[:, cut:] = res[ROWS : 2 * ROWS]
+        res = dot(low, w[:, :cut])
+        gs[1, :, :cut] = res[0:ROWS].astype(bf16)
+        send(gs.at[1, :, :cut], gr.at[1, :, :cut], s_, r_.at[4], yp)
+        kept[:, :cut] = res[ROWS : 2 * ROWS]
+        part[:, :cut] = res[2 * ROWS :]
+
+    def rs_mid(cut, a, w, xb, fs, fr, gs, gr, kept, s_, r_):
+        for k, (lo, hi, peer) in enumerate(((0, cut, yn), (cut, D, yp))):
+            got(fr.at[:, lo:hi], r_.at[2 + k], "w_f")
+            gs[k, :, lo:hi] = (part[:, lo:hi] + fr[:, lo:hi].astype(f32)).astype(bf16)
+            send(gs.at[k, :, lo:hi], gr.at[k, :, lo:hi], s_, r_.at[4], peer)
 
     def filtered(d, core):
         @pl.when(jnp.logical_and(jnp.logical_and(d == 0, core == 0), sp > 0))
@@ -315,8 +322,8 @@
         f = f + taps[2:3, mine] * near[8 : 8 + ROWS]
         cbr[rows, :] = (proj[rows, 1024:1280].astype(f32) * f).astype(bf16)
 
-    conv_set = (cbr, woc_v, x_c, fs_c, fr_c, gs_c, gr_c, own_c, rc_s, rc_r)
-    head_set = (mob, wom_v, x_h, fs_h, fr_h, gs_h, gr_h, own_h, rh_s, rh_r)
+    conv_set = (CUT, cbr, woc_v, x_c, fs_c, fr_c, gs_c, gr_c, own_c, rc_s, rc_r)
+    head_set = (COLS, mob, wom_v, x_h, fs_h, fr_h, gs_h, gr_h, own_h, rh_s, rh_r)
 
     def conv_part(n):
         rs_part(n, cbr, woc_v, x_c, rc_s, rc_r, filtered)
@@ -352,12 +359,12 @@
             every,
         )
         send_edge(0)
+    with scope("conv_early"):
+        conv_part(1)
     got(slots(12 + 2 * c), ag_r.at[2], "w_ag2")
     ag(12 + 2 * c, 12 + 2 * c, 11, sib)
     got(slots(13 + 2 * c), ag_r.at[5], "w_ag5")
     ag(13 + 2 * c, 13 + 2 * c, 12, sib)
-    with scope("conv_early"):
-        conv_part(1)
     keys, rest = ((1280, 1408), (0, 512)), ((512, 1024), (1024, 1280))
 
     def project_last(core, parts):
@@ -366,6 +373,9 @@
 
     with scope("proj_3own"):
         project_last(c, keys + rest)
+        pltpu.make_async_copy(woc_v, woc_v, wsem.at[1]).wait()
+        got(woc_v, ow_r)
+        rs_early(*conv_set)
     got(slots(0, 2), ag_r.at[9], "w_ag12")
     with scope("proj_3"):
         project_last(other, keys)
@@ -535,8 +545,6 @@
     with scope("rs_first_conv"):
         conv_part(0)
         conv_part(3)
-        pltpu.make_async_copy(woc_v, woc_v, wsem.at[1]).wait()
-        got(woc_v, ow_r)
         top = jnp.broadcast_to(u_row, (8, BLK))
         urow[...] = top
         for s in (1, 2, 4, 8, 16, 32, 64, 128, 256, 512):
@@ -575,7 +583,7 @@
 
     with scope("rs_second_conv"):
         conv_part(2)
-        rs_second(*conv_set)
+        rs_second(True, *conv_set)
 
     @pl.when(jnp.logical_not(last_group))
     def _():
@@ -624,12 +632,13 @@
         mob[rows, :] = memory_out.astype(bf16)
 
     with scope("rs_first_head"):
-        for n in (0, 1, 2):
+        for n in (0, 1):
             rs_part(n, mob, wom_v, x_h, rh_s, rh_r, heads)
         rs_first(*head_set)
     with scope("rs_second_head"):
-        rs_part(3, mob, wom_v, x_h, rh_s, rh_r, heads)
-        rs_second(*head_set)
+        for n in (2, 3):
+            rs_part(n, mob, wom_v, x_h, rh_s, rh_r, heads)
+        rs_second(False, *head_set)
     ss[me] = sqcol[...].T[0:1]
     for k in range(1, NTP):
         send(ss.at[me], ss.at[me], ss_s, ss_r, lax.rem(me + k, NTP))
@@ -645,14 +654,14 @@
     factor = scol[pl.ds(pl.multiple_of(me * ROWS, 8), ROWS), 0:1]
     for k in range(2):
         cs = slice(k * COLS, (k + 1) * COLS)
-        conv_sum = own_c[:, cs] + gr_c[k].astype(f32) + gr_c[2 + k].astype(f32)
+        conv_sum = own_c[:, cs] + gr_c[0, :, cs].astype(f32) + gr_c[1, :, cs].astype(f32)
         own_c[:, cs] = conv_sum + factor * own_h[:, cs]
     got(gr_h, rh_r.at[4], "w_gh")
     outs = []
     with scope("final"):
         for k in range(2):
             cs = slice(k * COLS, (k + 1) * COLS)
-            rest_sum = gr_h[k].astype(f32) + gr_h[2 + k].astype(f32)
+            rest_sum = gr_h[0, :, cs].astype(f32) + gr_h[1, :, cs].astype(f32)
             out[:, cs] = (own_c[:, cs] + factor * rest_sum).astype(bf16)
             outs.append(pltpu.make_async_copy(out.at[:, cs], out_h.at[:, cs], out_s.at[k]))
             outs[k].start()
@@ -702,10 +711,10 @@
     def rs_bufs():
         return [
             pltpu.VMEM((4, ROWS, CH), bf16),
-            pltpu.VMEM((2, ROWS, COLS), bf16),
-            pltpu.VMEM((2, ROWS, COLS), bf16),
-            pltpu.VMEM((4, ROWS, COLS), bf16),
-            pltpu.VMEM((4, ROWS, COLS), bf16),
+            pltpu.VMEM((ROWS, D), bf16),
+            pltpu.VMEM((ROWS, D), bf16),
+            pltpu.VMEM((2, ROWS, D), bf16),
+            pltpu.VMEM((2, ROWS, D), bf16),
         ]
 
     scratch = [
@@ -752,7 +761,7 @@
         pltpu.VMEM((BLK, 128), f32),
         pltpu.VMEM((ROWS, D), f32),
         pltpu.VMEM((ROWS, D), f32),
-        pltpu.VMEM((2, ROWS, COLS), f32),
+        pltpu.VMEM((ROWS, D), f32),
         pltpu.VMEM((ROWS, D), bf16),
         *rs_bufs(),
         *rs_bufs(),
@@ -764,9 +773,9 @@
         dma(()),
         dma(()),
         dma(()),
-        dma((5,)),
+        dma((6,)),
         dma(()),
-        dma((5,)),
+        dma((6,)),
         dma((2,)),
         dma(()),
         dma((2,)),

time: 57 us -> 56.8 us (level); the launches traced: 56.9 us -> 55.8 us
  Pallas kernels: 55.2 us -> 54 us
    pallas_call x1, Pallas kernels: 55.2 us -> 54 us  [per_device(): pl.pallas_call(functools.partial(kernel, n_sp), out_shape=jax.ShapeDtypeS...]
where the time goes in v6:
time: 56.8 us; the launch traced here: 55.8 us
  Pallas kernels  54 us (95%)
  local copies, waits for them, and re-layouts  1.77 us (3%)
    pallas_call x1, Pallas kernels, per_device(): pl.pallas_call(functools.partial(kernel, n_sp), out_shape=jax.ShapeDtypeS...  54 us
    unnamed x1, local copies, waits for them, and re-layouts  1.77 us

profile of v6, /device:TPU:1, one launch (start us, length us, event | category | flops | bytes accessed | tf_op | source)
XLA Modules:
  0.0 55.8 jit_solution(17388252360453399204)
XLA Ops:
  0.0 54.0 %shard_map.163 = bf16[96,2048]{1,0:T(8,128)(2,1)} custom-call(bf16[96,2048]{1,0:T(8,128)(2,1)} %tok_h.1, f32[1,2048]{1,0:T(1,128)} %bitcast.9, bf16[8,2048]{1,0:T(8,128)(2,1)} %bitcast.7, bf16[8,2048]{1,0:T(8,128)(2,1)} %bitcast.8, f32[1,8]{1,0:T(1,128)} %bitcast.11, f32[1,768]{1,0:T(1,128)} %bitcast.10, f32[3,2048]{1,0:T(4,128)} %taps_h.1, ...), custom_call_target="tpu_custom_call" | custom-call | tf_op jit(solution)/shard_map/pallas_call | solution.py:795
  54.0 1.8 %copy.19 = bf16[96,2048]{1,0:T(8,128)(2,1)} copy(bf16[96,2048]{1,0:T(8,128)(2,1)} %shard_map.163) | data formatting | bytes 786432
